TPU v7x, 256 devices: a whole 4x4x8 slice. The times are simulated.
256 devices in a mesh: sp: 32 (over z, x), tp: 8 (over y, core).
Axes of the slice: x: 4, y: 4, z: 8, core: 2. Of those that a mesh axis runs over, the one named last changes fastest.
Arguments:
- tokens: bfloat16 [2, 6144, 4096], P(None, 'sp', 'tp'), may hold values from -12 to 12
- query_weight: bfloat16 [4096, 2048], P(None, 'tp'), may hold values from -0.09375 to 0.09375
- key_weight: bfloat16 [4096, 2048], P(None, 'tp'), may hold values from -0.09375 to 0.09375
- value_weight: bfloat16 [4096, 2048], P(None, 'tp'), may hold values from -0.09375 to 0.09375
- gate_weight: bfloat16 [4096, 2048], P(None, 'tp'), may hold values from -0.09375 to 0.09375
- beta_weight: bfloat16 [4096, 16], P(None, 'tp'), may hold values from -0.09375 to 0.09375
- decay_weight: bfloat16 [4096, 16], P(None, 'tp'), may hold values from -0.09375 to 0.09375
- beta_bias: float32 [16], P('tp'), may hold values from -6 to -3
- rate_log: float32 [16], P('tp'), may hold values from -12 to -2.5
- out_gain: float32 [128], replicated, may hold values from 0.1 to 1.9
- new_query: bfloat16 [2, 16, 128], P(None, 'tp'), may hold values from -6 to 6
- new_key: bfloat16 [2, 16, 128], P(None, 'tp'), may hold values from -6 to 6
- new_value: bfloat16 [2, 16, 128], P(None, 'tp'), may hold values from -6 to 6
- new_beta: float32 [2, 16], P(None, 'tp'), may hold values from 0.1 to 0.9
- new_decay: float32 [2, 16], P(None, 'tp'), may hold values from 0.3 to 1
Outputs:
- mixed_out: bfloat16 [2, 6144, 2048], P(None, 'sp', 'tp')
- cache: bfloat16 [2, 16, 128, 128], P(None, 'tp', 'sp')
- first_out: float32 [2, 2048], P(None, 'tp')
All inputs are finite; a program needn't handle non-finite values.
Results may differ from a plain program's by a relative error of at most 0.0073.
Values may be sent and summed in bfloat16 or wider, within the bound.
A program may use at most 64 MiB of HBM per device.

v0:
```python
import functools

import jax
import jax.numpy as jnp
from jax import lax
from jax.experimental import pallas as pl
from jax.experimental.pallas import tpu as pltpu
from jax.sharding import PartitionSpec as P

unit_floor = 1.0
norm_floor = 0.001
highest = lax.Precision.HIGHEST
MESH = pl.DeviceIdType.MESH
PAD = 8
f32 = jnp.float32
bf16 = jnp.bfloat16

NN = (((1,), (0,)), ((), ()))
NT = (((1,), (1,)), ((), ()))
TN = (((0,), (0,)), ((), ()))


def dot(left, right, dims=NN, precision=None):
    return lax.dot_general(left, right, dims, precision=precision, preferred_element_type=f32)


def gather_kernel(
    n, seqs, x_ref, wq_ref, wk_ref, wv_ref, wg_ref, bw_ref, dw_ref, out_ref,
    small_ref, bd_ref, xs, wbuf, acc, sacc, wsem, cross_sem, part_sem, fwd_sem, rx,
):
    me = lax.axis_index("tp")
    y, c = me // 2, lax.rem(me, 2)
    chips = n // 2
    rows, kd = x_ref.shape
    span = rows // seqs
    _, chunks, _, kc = xs.shape
    partner = y * 2 + (1 - c)
    weights = (wq_ref, wk_ref, wv_ref, wg_ref)

    barrier = pltpu.get_barrier_semaphore()
    pl.semaphore_signal(barrier, inc=1, device_id={"tp": partner}, device_id_type=MESH)
    for d in range(1, chips):
        to = lax.rem(y + d, chips) * 2 + c
        pl.semaphore_signal(barrier, inc=1, device_id={"tp": to}, device_id_type=MESH)

    order = [me, partner]
    for d in range(1, chips):
        source = lax.rem(y - d + chips, chips)
        order += [source * 2 + c, source * 2 + (1 - c)]

    def weight_copy(w, slot):
        start = pl.multiple_of(order[slot] * kd, kd)
        return pltpu.make_async_copy(
            weights[w].at[pl.ds(start, kd), :], wbuf.at[w, slot], wsem.at[w, slot]
        )

    for slot in range(n):
        for w in range(4):
            weight_copy(w, slot).start()
    bd_ref[...] = jnp.zeros_like(bd_ref)
    bd_ref[0 : bw_ref.shape[0]] = bw_ref[...]
    bd_ref[PAD : PAD + dw_ref.shape[0]] = dw_ref[...]
    pl.semaphore_wait(barrier, chips)

    def cols(ck):
        return pl.ds(ck * kc, kc)

    def cross_copy(d, ck):
        to = lax.rem(y + d, chips) * 2 + c
        return pltpu.make_async_remote_copy(
            src_ref=x_ref.at[:, cols(ck)], dst_ref=xs.at[me, ck],
            send_sem=cross_sem.at[d - 1, ck], recv_sem=rx.at[me, ck],
            device_id={"tp": to}, device_id_type=MESH,
        )

    def part_copy(ck):
        return pltpu.make_async_remote_copy(
            src_ref=x_ref.at[:, cols(ck)], dst_ref=xs.at[me, ck],
            send_sem=part_sem.at[ck], recv_sem=rx.at[me, ck],
            device_id={"tp": partner}, device_id_type=MESH,
        )

    def fwd_copy(d, ck):
        b = order[2 * d]
        return pltpu.make_async_remote_copy(
            src_ref=xs.at[b, ck], dst_ref=xs.at[b, ck],
            send_sem=fwd_sem.at[d - 1, ck], recv_sem=rx.at[b, ck],
            device_id={"tp": partner}, device_id_type=MESH,
        )

    def arrive(b, ck):
        pltpu.make_async_remote_copy(
            src_ref=xs.at[b, ck], dst_ref=xs.at[b, ck],
            send_sem=part_sem.at[ck], recv_sem=rx.at[b, ck],
            device_id={"tp": partner}, device_id_type=MESH,
        ).wait_recv()

    for ck in range(chunks):
        for d in range(1, chips):
            cross_copy(d, ck).start()
    for ck in range(chunks):
        part_copy(ck).start()

    def small(x, start, depth, first):
        piece = bd_ref[:, pl.ds(pl.multiple_of(start, depth), depth)]
        for s in range(seqs):
            term = dot(piece, x[s * span : (s + 1) * span], NT)
            sacc[s] = term if first else sacc[s] + term

    for w in range(4):
        weight_copy(w, 0).wait()
        acc[w] = dot(x_ref[...], wbuf[w, 0])
    small(x_ref[...], me * kd, kd, True)

    def use(slot, ck):
        b = order[slot]
        x = xs[b, ck]
        for w in range(4):
            if ck == 0:
                weight_copy(w, slot).wait()
            acc[w] += dot(x, wbuf[w, slot, pl.ds(ck * kc, kc), :])
        small(x, b * kd + ck * kc, kc, False)

    for ck in range(chunks):
        arrive(partner, ck)
        use(1, ck)
    for d in range(1, chips):
        for ck in range(chunks):
            arrive(order[2 * d], ck)
            fwd_copy(d, ck).start()
            use(2 * d, ck)
            arrive(order[2 * d + 1], ck)
            use(2 * d + 1, ck)
    for w in range(4):
        out_ref[w] = acc[w].astype(bf16)
    small_ref[...] = sacc[...]
    for ck in range(chunks):
        part_copy(ck).wait_send()
        for d in range(1, chips):
            cross_copy(d, ck).wait_send()
            fwd_copy(d, ck).wait_send()


def gather_project(n, seqs, tokens, weights, bw, dw):
    rows, kd = tokens.shape
    width = weights[0].shape[1]
    kc = 256 if kd % 256 == 0 else kd
    chunks = kd // kc
    chips = n // 2
    span = rows // seqs
    return pl.pallas_call(
        functools.partial(gather_kernel, n, seqs),
        out_shape=(
            jax.ShapeDtypeStruct((4, rows, width), bf16),
            jax.ShapeDtypeStruct((seqs, 2 * PAD, span), f32),
        ),
        in_specs=[pl.BlockSpec(memory_space=pltpu.VMEM)]
        + [pl.BlockSpec(memory_space=pl.ANY)] * 4
        + [pl.BlockSpec(memory_space=pltpu.VMEM)] * 2,
        out_specs=(pl.BlockSpec(memory_space=pltpu.VMEM),) * 2,
        scratch_shapes=[
            pltpu.VMEM((2 * PAD, bw.shape[1]), bf16),
            pltpu.VMEM((n, chunks, rows, kc), bf16),
            pltpu.VMEM((4, n, kd, width), bf16),
            pltpu.VMEM((4, rows, width), f32),
            pltpu.VMEM((seqs, 2 * PAD, span), f32),
            pltpu.SemaphoreType.DMA((4, n)),
            pltpu.SemaphoreType.DMA((chips - 1, chunks)),
            pltpu.SemaphoreType.DMA((chunks,)),
            pltpu.SemaphoreType.DMA((chips - 1, chunks)),
            pltpu.SemaphoreType.DMA((n, chunks)),
        ],
        compiler_params=pltpu.CompilerParams(
            collective_id=0, has_side_effects=True, vmem_limit_bytes=60 * 1024 * 1024
        ),
    )(tokens, *weights, bw, dw)


def unit_rows(values):
    return values * lax.rsqrt(jnp.sum(values * values, axis=-1, keepdims=True) + unit_floor)


def delta_kernel(
    n, seqs, heads, group, rows_ref, small_ref, bias_ref, rate_ref, gain_ref, nq_ref, nk_ref, nv_ref,
    nb_ref, nd_ref, mixed_ref, cache_ref, first_ref,
    cum_row, cum_col, beta_col, local_out, reach, out_box, in_box, back_out, back_in, tail_out,
    tail_in, send1, recv1, send2, recv2, send3, recv3,
):
    me = lax.axis_index("sp")
    pairs = seqs * heads
    span = rows_ref.shape[1] // seqs
    extent = rows_ref.shape[2] // heads
    key_rows = extent // n

    barrier = pltpu.get_barrier_semaphore()
    for d in range(1, n):
        to = lax.rem(me + d, n)
        pl.semaphore_signal(barrier, inc=1, device_id={"sp": to}, device_id_type=MESH)

    row = lax.broadcasted_iota(jnp.int32, (span, span), 0)
    col = lax.broadcasted_iota(jnp.int32, (span, span), 1)
    upper = jnp.where(row <= col, 1.0, 0.0)
    slot_of = lax.broadcasted_iota(jnp.int32, (PAD, 1), 0)
    bias = jnp.zeros((PAD, 1), f32)
    rate = jnp.zeros((PAD, 1), f32)
    for h in range(heads):
        bias = jnp.where(slot_of == h, bias_ref[h], bias)
        rate = jnp.where(slot_of == h, rate_ref[h], rate)
    for s in range(seqs):
        beta = jax.nn.sigmoid(small_ref[s, 0:PAD, :] + bias)
        pre = small_ref[s, PAD : 2 * PAD, :]
        soft = jnp.maximum(pre, 0.0) + jnp.log1p(jnp.exp(-jnp.abs(pre)))
        cum = dot(-jnp.exp(rate) * soft, upper, NN, highest)
        cum_row[s] = cum
        cum_col[s] = cum.T
        beta_col[s] = beta.T
    eye_lane = lax.broadcasted_iota(jnp.int32, (extent, extent), 0) == lax.broadcasted_iota(
        jnp.int32, (extent, extent), 1
    )
    pl.semaphore_wait(barrier, n - 1)

    def send_box(p):
        return pltpu.make_async_remote_copy(
            src_ref=out_box.at[p], dst_ref=in_box.at[me],
            send_sem=send1.at[p], recv_sem=recv1.at[me],
            device_id={"sp": p}, device_id_type=MESH,
        )

    def local_group(i, _):
        ps = [lax.rem(me + 1 + i * group + j, pairs) for j in range(group)]
        each = []
        for p in ps:
            s, h = p // heads, lax.rem(p, heads)
            at = pl.ds(pl.multiple_of(s * span, span), span)
            lanes = pl.ds(pl.multiple_of(h * extent, extent), extent)
            q = unit_rows(rows_ref[0, at, lanes].astype(f32))
            k = unit_rows(rows_ref[1, at, lanes].astype(f32))
            v = rows_ref[2, at, lanes].astype(f32)
            pick = lax.broadcasted_iota(jnp.int32, (span, PAD), 1) == h
            cumc = jnp.sum(jnp.where(pick, cum_col[s], 0.0), axis=1, keepdims=True)
            beta = jnp.sum(jnp.where(pick, beta_col[s], 0.0), axis=1, keepdims=True)
            cumr = cum_row[s, pl.ds(h, 1), :]
            causal = row >= col
            weights = jnp.where(causal, jnp.exp(jnp.where(causal, cumc - cumr, 0.0)), 0.0)
            kb = k * beta
            kh = k.astype(bf16)
            lower = jnp.where(row > col, dot(kb.astype(bf16), kh, NT) * weights, 0.0)
            score = (dot(q.astype(bf16), kh, NT) * weights).astype(bf16)
            grow = jnp.exp(cumc)
            right = jnp.concatenate([v * beta, kb * grow], axis=1).astype(bf16)
            last = cumc[span - 1 :, :]
            kdec = (k * jnp.exp(last - cumc)).astype(bf16)
            each.append([lower, score, right, kdec, q * grow, jnp.exp(last)])
        unit = jnp.where(row == col, 1.0, 0.0)
        pair_mask = ((row >> 1) == (col >> 1)) & (row > col)
        inv = [unit - jnp.where(pair_mask, e[0], 0.0) for e in each]
        level = 1
        while (1 << level) < span:
            mask = ((row >> (level + 1)) == (col >> (level + 1))) & ((row >> level) > (col >> level))
            inv_h = [m.astype(bf16) for m in inv]
            mid = [
                dot(jnp.where(mask, e[0], 0.0).astype(bf16), m).astype(bf16)
                for e, m in zip(each, inv_h)
            ]
            inv = [m - dot(mh, t) for m, mh, t in zip(inv, inv_h, mid)]
            level += 1
        uw = [dot(m.astype(bf16), e[2]).astype(bf16) for m, e in zip(inv, each)]
        out = [dot(e[1], u) for e, u in zip(each, uw)]
        fin = [dot(e[3], u, TN) for e, u in zip(each, uw)]
        for p, e, o, z in zip(ps, each, out, fin):
            local_out[p] = o[:, :extent]
            reach[p] = (e[4] - o[:, extent:]).astype(bf16)
            step = (jnp.where(eye_lane, e[5] - 1.0, 0.0) - z[:, extent:]).astype(bf16)
            state = z[:, :extent].astype(bf16)

            @pl.when(p == me)
            def _():
                in_box[me, 0] = step
                in_box[me, 1] = state

            @pl.when(p != me)
            def _():
                out_box[p, 0] = step
                out_box[p, 1] = state
                send_box(p).start()

        return 0

    lax.fori_loop(0, pairs // group, local_group, 0)

    def back_copy(j):
        return pltpu.make_async_remote_copy(
            src_ref=back_out.at[j], dst_ref=back_in.at[me],
            send_sem=send2.at[j], recv_sem=recv2.at[me],
            device_id={"sp": j}, device_id_type=MESH,
        )

    def tail_copy(j):
        return pltpu.make_async_remote_copy(
            src_ref=tail_out.at[j], dst_ref=tail_in.at[me],
            send_sem=send3.at[j], recv_sem=recv3.at[me],
            device_id={"sp": j}, device_id_type=MESH,
        )

    @pl.when(me < pairs)
    def _():
        def chain(j, state):
            half = state.astype(bf16)

            @pl.when(j == me)
            def _():
                back_in[me] = half

            @pl.when(j != me)
            def _():
                back_out[j] = half
                back_copy(j).start()
                pltpu.make_async_remote_copy(
                    src_ref=out_box.at[0], dst_ref=in_box.at[j],
                    send_sem=send1.at[0], recv_sem=recv1.at[j],
                    device_id={"sp": j}, device_id_type=MESH,
                ).wait_recv()

            return state + dot(in_box[j, 0], half) + in_box[j, 1].astype(f32)

        final = lax.fori_loop(0, n, chain, jnp.zeros((extent, extent), f32))
        memory = final.astype(bf16).astype(f32)
        shape3 = nq_ref.shape
        mine = (
            lax.broadcasted_iota(jnp.int32, shape3, 0) * heads
            + lax.broadcasted_iota(jnp.int32, shape3, 1)
        ) == me

        def own(ref):
            kept = jnp.where(mine, ref[...].astype(f32), 0.0)
            return jnp.sum(jnp.sum(kept, axis=0), axis=0, keepdims=True)

        qn, kn = unit_rows(own(nq_ref)), unit_rows(own(nk_ref))
        both = jnp.concatenate([jnp.broadcast_to(qn, (PAD, extent)), jnp.broadcast_to(kn, (PAD, extent))], axis=0)
        reads = dot(both, memory, NN, highest)
        recall, retrieve = reads[0:1], reads[PAD : PAD + 1]
        s, h = me // heads, lax.rem(me, heads)
        beta_new, decay_new = nb_ref[s, h], nd_ref[s, h]
        fresh = own(nv_ref) - decay_new * retrieve
        meet = jnp.sum(kn * qn, axis=-1, keepdims=True)
        read = decay_new * recall + (beta_new * meet) * fresh
        norm = lax.rsqrt(jnp.mean(read * read, axis=-1, keepdims=True) + norm_floor)
        answer = jnp.broadcast_to(read * norm * gain_ref[...], (PAD, extent))
        for j in range(n):
            tail_out[j, 0:key_rows, :] = memory[j * key_rows : (j + 1) * key_rows]
            tail_out[j, tail_out.shape[1] - PAD :, :] = answer

        def push(j, _):
            @pl.when(j == me)
            def _():
                tail_in[me] = tail_out[me]

            @pl.when(j != me)
            def _():
                tail_copy(j).start()

            return 0

        lax.fori_loop(0, n, push, 0)

    gain = gain_ref[...]

    def finish(i, _):
        p = lax.rem(me + i, pairs)
        s, h = p // heads, lax.rem(p, heads)
        at = pl.ds(pl.multiple_of(s * span, span), span)
        lanes = pl.ds(pl.multiple_of(h * extent, extent), extent)

        @pl.when(p != me)
        def _():
            pltpu.make_async_remote_copy(
                src_ref=back_out.at[0], dst_ref=back_in.at[p],
                send_sem=send2.at[0], recv_sem=recv2.at[p],
                device_id={"sp": p}, device_id_type=MESH,
            ).wait_recv()

        o = local_out[p] + dot(reach[p], back_in[p])
        norm = lax.rsqrt(jnp.mean(o * o, axis=-1, keepdims=True) + norm_floor)
        gate = rows_ref[3, at, lanes].astype(f32)
        mixed_ref[at, lanes] = (o * norm * gain * (gate * jax.nn.sigmoid(gate))).astype(bf16)
        return 0

    lax.fori_loop(0, pairs, finish, 0)

    for p in range(pairs):

        @pl.when(p != me)
        def _():
            pltpu.make_async_remote_copy(
                src_ref=tail_out.at[0], dst_ref=tail_in.at[p],
                send_sem=send3.at[0], recv_sem=recv3.at[p],
                device_id={"sp": p}, device_id_type=MESH,
            ).wait_recv()

        cache_ref[p] = tail_in[p, 0:key_rows, :].astype(bf16)
        last = tail_in.shape[1]
        first_ref[p : p + 1, :] = tail_in[p, last - PAD : last - PAD + 1, :]

    for p in range(pairs):

        @pl.when(p != me)
        def _():
            send_box(p).wait_send()

    @pl.when(me < pairs)
    def _():
        for j in range(n):

            @pl.when(j != me)
            def _():
                back_copy(j).wait_send()
                tail_copy(j).wait_send()


def delta(n, seqs, heads, rows4, small, bias, rate, gain, nq, nk, nv, nb, nd):
    _, rows, width = rows4.shape
    span, extent = rows // seqs, width // heads
    pairs = seqs * heads
    key_rows = extent // n
    tail = -(-key_rows // PAD) * PAD + PAD
    vmem = pl.BlockSpec(memory_space=pltpu.VMEM)
    smem = pl.BlockSpec(memory_space=pltpu.SMEM)
    return pl.pallas_call(
        functools.partial(delta_kernel, n, seqs, heads, 2),
        out_shape=(
            jax.ShapeDtypeStruct((rows, width), bf16),
            jax.ShapeDtypeStruct((pairs, key_rows, extent), bf16),
            jax.ShapeDtypeStruct((pairs, extent), f32),
        ),
        in_specs=[vmem] * 2 + [smem] * 2 + [vmem] * 4 + [smem] * 2,
        out_specs=(vmem,) * 3,
        scratch_shapes=[
            pltpu.VMEM((seqs, PAD, span), f32),
            pltpu.VMEM((seqs, span, PAD), f32),
            pltpu.VMEM((seqs, span, PAD), f32),
            pltpu.VMEM((pairs, span, extent), f32),
            pltpu.VMEM((pairs, span, extent), bf16),
            pltpu.VMEM((pairs, 2, extent, extent), bf16),
            pltpu.VMEM((n, 2, extent, extent), bf16),
            pltpu.VMEM((n, extent, extent), bf16),
            pltpu.VMEM((pairs, extent, extent), bf16),
            pltpu.VMEM((n, tail, extent), f32),
            pltpu.VMEM((pairs, tail, extent), f32),
            pltpu.SemaphoreType.DMA((pairs,)),
            pltpu.SemaphoreType.DMA((n,)),
            pltpu.SemaphoreType.DMA((n,)),
            pltpu.SemaphoreType.DMA((pairs,)),
            pltpu.SemaphoreType.DMA((n,)),
            pltpu.SemaphoreType.DMA((pairs,)),
        ],
        compiler_params=pltpu.CompilerParams(
            collective_id=1, has_side_effects=True, vmem_limit_bytes=48 * 1024 * 1024
        ),
    )(rows4, small, bias, rate, gain, nq, nk, nv, nb, nd)


def shards(
    tokens, query_weight, key_weight, value_weight, gate_weight, beta_weight, decay_weight,
    beta_bias, rate_log, out_gain, new_query, new_key, new_value, new_beta, new_decay,
):
    seqs, span, kd = tokens.shape
    heads = rate_log.shape[0]
    extent = out_gain.shape[0]
    tp, sp = lax.axis_size("tp"), lax.axis_size("sp")
    weights = (query_weight, key_weight, value_weight, gate_weight)
    rows4, small = gather_project(tp, seqs, tokens.reshape(seqs * span, kd), weights, beta_weight.T, decay_weight.T)
    mixed, cache, first = delta(
        sp, seqs, heads, rows4, small, beta_bias, rate_log, out_gain[None], new_query, new_key, new_value,
        new_beta, new_decay,
    )
    return (
        mixed.reshape(seqs, span, heads * extent),
        cache.reshape(seqs, heads, extent // sp, extent),
        first.reshape(seqs, heads * extent),
    )


def solution(mesh):
    placed = (
        P(None, "sp", "tp"),
        P(None, "tp"),
        P(None, "tp"),
        P(None, "tp"),
        P(None, "tp"),
        P(None, "tp"),
        P(None, "tp"),
        P("tp"),
        P("tp"),
        P(),
        P(None, "tp", None),
        P(None, "tp", None),
        P(None, "tp", None),
        P(None, "tp"),
        P(None, "tp"),
    )
    return jax.shard_map(
        shards,
        mesh=mesh,
        in_specs=placed,
        out_specs=(P(None, "sp", "tp"), P(None, "tp", "sp", None), P(None, "tp")),
        check_vma=False,
    )
```

profile of v0, /device:TPU:1, one launch (start us, length us, event | category | flops | bytes accessed | tf_op | source)
XLA Modules:
  0.0 89.4 jit_solution(9986169187605424161)
XLA Ops:
  0.6 0.0 copy-start.2
  0.6 0.0 copy-start.3
  0.7 0.0 copy-start.4
  0.7 0.0 copy-start.5
  0.7 0.0 copy-start.6
  0.7 0.0 copy-start.7
  0.7 0.0 copy-start.8
  0.7 0.0 copy-start.9
  0.7 31.2 %shard_map.166 = (bf16[4,384,256]{2,1,0:T(8,128)(2,1)}, f32[2,16,192]{2,1,0:T(8,128)}) custom-call(bf16[384,512]{1,0:T(8,128)(2,1)} %bitcast.9, bf16[4096,256]{1,0:T(8,128)(2,1)} %wq_ref.1, bf16[4096,256]{1,0:T(8,128)(2,1)} %wk_ref.1, bf16[4096,256]{1,0:T(8,128)(2,1)} %wv_ref.1, bf16[4096,256]{1,0:T(8,128)(2,1)} %wg_ref.1, bf16[2,4096]{1,0:T(2,128)(2,1)} %bitcast.10, ...), custom_call_target="tpu_custom_call" | custom-call | tf_op jit(solution)/shard_map/pallas_call | solution.py:151
  32.0 0.0 copy-done.2
  32.0 0.0 copy-done.3
  32.0 0.0 copy-done.4
  32.0 0.0 copy-done.5
  32.0 0.0 copy-done.6
  32.0 0.0 copy-done.7
  32.0 0.0 copy-done.8
  32.0 0.0 copy-done.9
  32.0 0.0 copy-start
  32.1 1.1 %copy-done = bf16[4,384,256]{2,1,0:T(8,128)(2,1)S(1)} copy-done((bf16[4,384,256]{2,1,0:T(8,128)(2,1)S(1)}, bf16[4,384,256]{2,1,0:T(8,128)(2,1)}, u32[]{:S(2)}) %copy-start) | copy-done | bytes 786456
  33.2 0.0 copy-start.1
  33.2 0.8 copy-done.1
  33.9 53.6 %shard_map.167 = (bf16[384,256]{1,0:T(8,128)(2,1)S(1)}, bf16[4,4,128]{2,1,0:T(4,128)(2,1)S(1)}, f32[4,128]{1,0:T(4,128)S(1)}) custom-call(bf16[4,384,256]{2,1,0:T(8,128)(2,1)S(1)} %copy-done, f32[2,16,192]{2,1,0:T(8,128)S(1)} %copy-done.1, f32[2]{0:T(128)S(1)} %copy-done.7, f32[2]{0:T(128)S(1)} %copy-done.8, f32[1,128]{1,0:T(1,128)S(1)} %bitcast.8, ...), custom_call_target="tpu_custom_call" | custom-call | tf_op jit(solution)/shard_map/pallas_call | solution.py:428
  87.5 0.6 reshape.21
  88.1 0.7 copy.20
  88.8 0.6 copy.21
Async XLA Ops:
  0.6 31.3 %copy-start.2 = (bf16[2,2,128]{2,1,0:T(2,128)(2,1)S(1)}, bf16[2,2,128]{2,1,0:T(2,128)(2,1)}, u32[]{:S(2)}) copy-start(bf16[2,2,128]{2,1,0:T(2,128)(2,1)} %nq_ref.1) | copy-start | bytes 3076
  0.6 31.3 %copy-start.3 = (bf16[2,2,128]{2,1,0:T(2,128)(2,1)S(1)}, bf16[2,2,128]{2,1,0:T(2,128)(2,1)}, u32[]{:S(2)}) copy-start(bf16[2,2,128]{2,1,0:T(2,128)(2,1)} %nk_ref.1) | copy-start | bytes 3076
  0.7 31.3 %copy-start.4 = (bf16[2,2,128]{2,1,0:T(2,128)(2,1)S(1)}, bf16[2,2,128]{2,1,0:T(2,128)(2,1)}, u32[]{:S(2)}) copy-start(bf16[2,2,128]{2,1,0:T(2,128)(2,1)} %nv_ref.1) | copy-start | bytes 3076
  0.7 31.3 %copy-start.5 = (f32[2,2]{1,0:T(2,128)S(1)}, f32[2,2]{1,0:T(2,128)}, u32[]{:S(2)}) copy-start(f32[2,2]{1,0:T(2,128)} %nb_ref.1) | copy-start | bytes 52
  0.7 31.3 %copy-start.6 = (f32[2,2]{1,0:T(2,128)S(1)}, f32[2,2]{1,0:T(2,128)}, u32[]{:S(2)}) copy-start(f32[2,2]{1,0:T(2,128)} %nd_ref.1) | copy-start | bytes 52
  0.7 31.3 %copy-start.7 = (f32[2]{0:T(128)S(1)}, f32[2]{0:T(128)}, u32[]{:S(2)}) copy-start(f32[2]{0:T(128)} %bias_ref.1) | copy-start | bytes 28
  0.7 31.3 %copy-start.8 = (f32[2]{0:T(128)S(1)}, f32[2]{0:T(128)}, u32[]{:S(2)}) copy-start(f32[2]{0:T(128)} %rate_ref.1) | copy-start | bytes 28
  0.7 31.3 %copy-start.9 = (f32[128]{0:T(128)S(1)}, f32[128]{0:T(128)}, u32[]{:S(2)}) copy-start(f32[128]{0:T(128)} %param.24) | copy-start | bytes 1540
  32.0 1.1 %copy-start = (bf16[4,384,256]{2,1,0:T(8,128)(2,1)S(1)}, bf16[4,384,256]{2,1,0:T(8,128)(2,1)}, u32[]{:S(2)}) copy-start(bf16[4,384,256]{2,1,0:T(8,128)(2,1)} %get-tuple-element.8.rows_ref) | copy-start | bytes 2359300
  33.2 0.8 copy-start.1
where the time goes:
time: 90.5 us; the launch traced here: 89.4 us
  Pallas kernels  84.8 us (94%)
  local copies, waits for them, and re-layouts  3.78 us (4%)
    pallas_call x1, Pallas kernels, delta(): pl.pallas_call(functools.partial(delta_kernel, n, seqs, heads, 2), out_sh...  53.6 us
    pallas_call x1, Pallas kernels, gather_project(): pl.pallas_call(functools.partial(gather_kernel, n, seqs), out_shape=(jax....  31.2 us
    unnamed x22, local copies, waits for them, and re-layouts  3.19 us

commit v1 on v0

v1 whole, which is shorter than its diff:
```python
import types

import jax
import jax.numpy as jnp
from jax import lax
from jax.experimental import pallas as pl
from jax.experimental.pallas import tpu as pltpu
from jax.sharding import PartitionSpec as P

unit_floor = 1.0
norm_floor = 0.001
highest = lax.Precision.HIGHEST
MESH = pl.DeviceIdType.MESH
PAD = 8
GROUP = 4
BLOCK = 64
f32 = jnp.float32
bf16 = jnp.bfloat16

NN = (((1,), (0,)), ((), ()))
NT = (((1,), (1,)), ((), ()))
TN = (((0,), (0,)), ((), ()))


def dot(left, right, dims=NN, precision=None):
    return lax.dot_general(left, right, dims, precision=precision, preferred_element_type=f32)


def half(values):
    return values.astype(bf16)


def unit_rows(values):
    return values * lax.rsqrt(jnp.sum(values * values, axis=-1, keepdims=True) + unit_floor)


def iota(shape, dim):
    return lax.broadcasted_iota(jnp.int32, shape, dim)


def unit_lower_inverses(blocks):
    size = blocks[0].shape[0]
    row, col = iota((size, size), 0), iota((size, size), 1)
    unit = jnp.where(row == col, 1.0, 0.0)
    pair = ((row >> 1) == (col >> 1)) & (row > col)
    inv = [unit - jnp.where(pair, b, 0.0) for b in blocks]
    level = 1
    while (1 << level) < size:
        mask = ((row >> (level + 1)) == (col >> (level + 1))) & ((row >> level) > (col >> level))
        inv_h = [half(m) for m in inv]
        mid = [half(dot(half(jnp.where(mask, b, 0.0)), m)) for b, m in zip(blocks, inv_h)]
        inv = [m - dot(mh, t) for m, mh, t in zip(inv, inv_h, mid)]
        level += 1
    return [half(m) for m in inv]


def fused_kernel(names, dims, *refs):
    r = types.SimpleNamespace(**dict(zip(names, refs)))
    seqs, heads, span, extent, kc = dims
    hv = extent // 2
    box = extent + hv
    nblk = span // BLOCK

    me = lax.axis_index("tp")
    y, c = me // 2, lax.rem(me, 2)
    sp = lax.axis_index("sp")
    z, x = sp // GROUP, lax.rem(sp, GROUP)
    zl = lax.rem(z, GROUP)
    lower_quad = z < GROUP
    partner = y * 2 + (1 - c)

    def tid(dy, core):
        return lax.rem(y + dy + 4, 4) * 2 + core

    nxt, prv, opp = tid(1, c), tid(-1, c), tid(2, c)
    order = [me, partner, prv, tid(-1, 1 - c), nxt, tid(1, 1 - c), opp, tid(2, 1 - c)]
    kd = 2 * kc
    weights = (r.wq, r.wk, r.wv, r.wg)

    def sp_id(zz, xx):
        return {"sp": zz * GROUP + xx}

    def peer_x(d):
        return lax.rem(x + d, GROUP)

    def peer_zl(d):
        return lax.rem(zl + d, GROUP)

    def peer_z(d):
        return z - zl + peer_zl(d)

    barrier = pltpu.get_barrier_semaphore()

    def greet(device):
        pl.semaphore_signal(barrier, inc=1, device_id=device, device_id_type=MESH)

    for t in (nxt, prv, partner):
        greet({"tp": t})
    for d in range(1, GROUP):
        greet(sp_id(z, peer_x(d)))
        greet(sp_id(peer_z(d), x))

    is_a, is_b = z == GROUP - 1, z == 0
    spreads = jnp.logical_or(is_a, is_b)

    def spread_to(k):
        return jnp.where(is_a, GROUP + k, 2 * GROUP - 1 - k)

    @pl.when(spreads)
    def _():
        for k in range(2):
            greet(sp_id(spread_to(k), x))

    spread_from = jnp.where(z < GROUP + 2, GROUP - 1, 0)

    @pl.when(jnp.logical_not(lower_quad))
    def _():
        greet(sp_id(spread_from, x))

    def token_copy(s, hf):
        return pltpu.make_async_copy(
            r.x.at[s, :, pl.ds(hf * kc, kc)], r.xs.at[me, s, hf], r.tok_sem.at[s, hf]
        )

    for s in range(seqs):
        for hf in range(2):
            token_copy(s, hf).start()

    def weight_copy(w, slot):
        start = pl.multiple_of(order[slot] * kd, kd)
        return pltpu.make_async_copy(weights[w].at[pl.ds(start, kd), :], r.wbuf.at[w, slot], r.wsem.at[w, slot])

    for slot in range(8):
        for w in range(4):
            weight_copy(w, slot).start()
    r.bd[...] = jnp.zeros_like(r.bd)
    r.bd[0:heads] = r.bw[...]
    r.bd[PAD : PAD + heads] = r.dw[...]
    extra = jnp.where(spreads, 2, jnp.where(lower_quad, 0, 1))
    pl.semaphore_wait(barrier, 3 + 2 * (GROUP - 1) + extra)

    def ring(b, s, hf, to, sem):
        return pltpu.make_async_remote_copy(
            src_ref=r.xs.at[b, s, hf], dst_ref=r.xs.at[b, s, hf], send_sem=sem,
            recv_sem=r.rx.at[b, s, hf], device_id={"tp": to}, device_id_type=MESH,
        )

    def own_sends(s):
        return [
            ring(me, s, 0, nxt, r.own_sem.at[0, s, 0]),
            ring(me, s, 1, prv, r.own_sem.at[1, s, 1]),
            ring(me, s, 1, nxt, r.own_sem.at[0, s, 1]),
            ring(me, s, 0, prv, r.own_sem.at[1, s, 0]),
            ring(me, s, 0, partner, r.part_sem.at[0, s, 0]),
            ring(me, s, 1, partner, r.part_sem.at[0, s, 1]),
        ]

    def forward(s, i):
        return ring((prv, nxt)[i], s, i, (nxt, prv)[i], r.fwd_sem.at[i, s])

    def partner_send(s, i, hf):
        return ring((prv, nxt, opp)[i], s, hf, partner, r.part_sem.at[1 + i, s, hf])

    def arrive(b, s, hf):
        ring(b, s, hf, partner, r.part_sem.at[0, s, hf]).wait_recv()

    def use(s, items, first=False):
        parts = [r.xs[order[slot], s, hf] for slot, hf in items]
        if s == 0:
            for slot in sorted({slot for slot, hf in items} - set(waited)):
                waited.append(slot)
                for w in range(4):
                    weight_copy(w, slot).wait()
        for w in range(4):
            total = None
            for (slot, hf), part in zip(items, parts):
                term = dot(part, r.wbuf[w, slot, hf * kc : (hf + 1) * kc, :])
                total = term if total is None else total + term
            r.acc[w] = total if first else r.acc[w] + total
        total = None
        for (slot, hf), part in zip(items, parts):
            piece = r.bd[:, pl.ds(pl.multiple_of(order[slot] * kd + hf * kc, kc), kc)]
            term = dot(piece, part, NT)
            total = term if total is None else total + term
        r.sacc[...] = total if first else r.sacc[...] + total

    waited = []

    def start_own(s):
        for hf in range(2):
            token_copy(s, hf).wait()
        for copy in own_sends(s):
            copy.start()

    def first_arrivals(s):
        arrive(prv, s, 0)
        forward(s, 0).start()
        arrive(nxt, s, 1)
        forward(s, 1).start()
        partner_send(s, 0, 0).start()
        partner_send(s, 1, 1).start()

    def rest(s):
        arrive(order[3], s, 0)
        arrive(order[5], s, 1)
        use(s, [(3, 0), (5, 1)])
        arrive(prv, s, 1)
        partner_send(s, 0, 1).start()
        arrive(nxt, s, 0)
        partner_send(s, 1, 0).start()
        use(s, [(2, 1), (4, 0)])
        arrive(order[3], s, 1)
        arrive(order[5], s, 0)
        use(s, [(3, 1), (5, 0)])
        arrive(opp, s, 0)
        partner_send(s, 2, 0).start()
        arrive(opp, s, 1)
        partner_send(s, 2, 1).start()
        use(s, [(6, 0), (6, 1)])
        arrive(order[7], s, 0)
        arrive(order[7], s, 1)
        use(s, [(7, 0), (7, 1)])
        for w in range(4):
            r.rows[s, w] = half(r.acc[w])

    def near(s):
        use(s, [(0, 0), (0, 1)], True)
        for hf in range(2):
            arrive(partner, s, hf)
        use(s, [(1, 0), (1, 1)])


    slot_of = iota((PAD, 1), 0)
    bias = jnp.zeros((PAD, 1), f32)
    rate = jnp.zeros((PAD, 1), f32)
    for h in range(heads):
        bias = jnp.where(slot_of == h, r.bias[h], bias)
        rate = jnp.where(slot_of == h, r.rate[h], rate)

    def x_copy(s, o):
        return pltpu.make_async_remote_copy(
            src_ref=r.out1.at[s, o], dst_ref=r.in1.at[s, x], send_sem=r.send1.at[s, o],
            recv_sem=r.recv1.at[s, x], device_id=sp_id(z, o), device_id_type=MESH,
        )

    def local(s, hook):
        upper = jnp.where(iota((span, span), 0) <= iota((span, span), 1), 1.0, 0.0)
        beta8 = jax.nn.sigmoid(r.sacc[0:PAD] + bias)
        pre = r.sacc[PAD : 2 * PAD]
        soft = jnp.maximum(pre, 0.0) + jnp.log1p(jnp.exp(-jnp.abs(pre)))
        cum8 = dot(-jnp.exp(rate) * soft, upper, NN, highest)
        cum_t, beta_t = cum8.T, beta8.T
        row, col = iota((BLOCK, BLOCK), 0), iota((BLOCK, BLOCK), 1)
        causal = row >= col
        per_head = []
        diags = []
        for h in range(heads):
            lanes = slice(h * extent, (h + 1) * extent)
            q = unit_rows(r.rows[s, 0, :, lanes].astype(f32))
            k = unit_rows(r.rows[s, 1, :, lanes].astype(f32))
            v = r.rows[s, 2, :, lanes].astype(f32)
            cumc, beta = cum_t[:, h : h + 1], beta_t[:, h : h + 1]
            cumr = cum8[h : h + 1, :]
            kb = k * beta
            qh, kh, kbh = half(q), half(k), half(kb)
            grow = jnp.exp(cumc)
            last = cumc[span - 1 :, :]
            right = jnp.concatenate([v * beta, kb * grow], axis=1)
            low_off, sc_diag, sc_off = [], [], []
            for i in range(nblk):
                at = slice(i * BLOCK, (i + 1) * BLOCK)
                diff = cumc[at] - cumr[:, at]
                w_d = jnp.where(causal, jnp.exp(jnp.where(causal, diff, 0.0)), 0.0)
                diags.append(jnp.where(row > col, dot(kbh[at], kh[at], NT) * w_d, 0.0))
                sc_diag.append(half(dot(qh[at], kh[at], NT) * w_d))
                if i:
                    before = slice(0, i * BLOCK)
                    w_o = jnp.exp(cumc[at] - cumr[:, before])
                    low_off.append(half(dot(kbh[at], kh[before], NT) * w_o))
                    sc_off.append(half(dot(qh[at], kh[before], NT) * w_o))
            per_head.append(
                dict(right=right, low=low_off, scd=sc_diag, sco=sc_off, qg=q * grow, last=last,
                     kdec=half(k * jnp.exp(last - cumc)))
            )
        hook()
        inv = unit_lower_inverses(diags)
        done = [[] for _ in range(heads)]
        for i in range(nblk):
            at = slice(i * BLOCK, (i + 1) * BLOCK)
            for h in range(heads):
                e = per_head[h]
                rhs = e["right"][at]
                if i:
                    rhs = rhs - dot(e["low"][i - 1], jnp.concatenate(done[h], axis=0) if i > 1 else done[h][0])
                done[h].append(half(dot(inv[h * nblk + i], half(rhs))))
        eye = iota((extent, extent), 0) == iota((extent, extent), 1)
        for h in range(heads):
            e = per_head[h]
            uw = jnp.concatenate(done[h], axis=0)
            fin = dot(uw, e["kdec"], TN)
            step = half(jnp.where(eye, jnp.exp(e["last"]) - 1.0, 0.0) - fin[extent:])
            state = half(fin[:extent])
            for f in range(2):
                r.out1[s, 2 * h + f, 0:extent, :] = step
                r.out1[s, 2 * h + f, extent:, :] = state[f * hv : (f + 1) * hv]
        for o in range(GROUP):

            @pl.when(x != o)
            def _():
                x_copy(s, o).start()

            @pl.when(x == o)
            def _():
                r.in1[s, x] = r.out1[s, o]

        for h in range(heads):
            e = per_head[h]
            for i in range(nblk):
                at = slice(i * BLOCK, (i + 1) * BLOCK)
                out = dot(e["scd"][i], done[h][i])
                if i:
                    out = out + dot(e["sco"][i - 1], jnp.concatenate(done[h][:i], axis=0) if i > 1 else done[h][0])
                r.local_out[s, h, at, :] = out[:, :extent]
                r.reach[s, h, at, :] = half(e["qg"][at] - out[:, extent:])
            gate = r.rows[s, 3, :, h * extent : (h + 1) * extent].astype(f32)
            r.gated[s, h] = gate * jax.nn.sigmoid(gate) * r.gain[...]


    def compose(prefix, step):
        e = step[0:extent]
        return prefix + dot(half(prefix), e) + step.astype(f32)

    def quad_copy(s, d):
        return pltpu.make_async_remote_copy(
            src_ref=r.in2.at[s, zl], dst_ref=r.in2.at[s, zl], send_sem=r.send2.at[s, d - 1],
            recv_sem=r.recv2.at[s, zl], device_id=sp_id(peer_z(d), x), device_id_type=MESH,
        )

    def combine_group(s):
        for j in range(GROUP):

            @pl.when(x != j)
            def _():
                pltpu.make_async_remote_copy(
                    src_ref=r.out1.at[s, 0], dst_ref=r.in1.at[s, j], send_sem=r.send1.at[s, 0],
                    recv_sem=r.recv1.at[s, j], device_id=sp_id(z, j), device_id_type=MESH,
                ).wait_recv()

        prefix = r.in1[s, 0].astype(f32)
        for j in range(1, GROUP):
            r.gpre[s, j - 1] = prefix
            prefix = compose(prefix, r.in1[s, j])
        r.in2[s, zl] = half(prefix)
        for d in (3, 2, 1):
            quad_copy(s, d).start()

    def spread_copy(s, k):
        return pltpu.make_async_remote_copy(
            src_ref=r.s4_out.at[s], dst_ref=r.s4_in.at[s], send_sem=r.send3.at[s, k],
            recv_sem=r.recv3.at[s], device_id=sp_id(spread_to(k), x), device_id_type=MESH,
        )

    def state_copy(s, xx):
        return pltpu.make_async_remote_copy(
            src_ref=r.st_out.at[s, xx], dst_ref=r.st_in.at[s, x], send_sem=r.send4.at[s, xx],
            recv_sem=r.recv4.at[s, x], device_id=sp_id(z, xx), device_id_type=MESH,
        )

    def give_states(s, states):
        for xx in range(GROUP):
            r.st_out[s, xx] = half(states[xx])
        for xx in range(GROUP):

            @pl.when(x != xx)
            def _():
                state_copy(s, xx).start()

            @pl.when(x == xx)
            def _():
                r.st_in[s, x] = r.st_out[s, xx]

    def combine_quad(s):
        for d in range(1, GROUP):
            j = peer_zl(d)
            pltpu.make_async_remote_copy(
                src_ref=r.in2.at[s, j], dst_ref=r.in2.at[s, j], send_sem=r.send2.at[s, 0],
                recv_sem=r.recv2.at[s, j], device_id=sp_id(peer_z(d), x), device_id_type=MESH,
            ).wait_recv()
        r.qpre[0] = jnp.zeros((box, extent), f32)
        prefix = r.in2[s, 0].astype(f32)
        r.qpre[1] = prefix
        for j in range(1, GROUP):
            prefix = compose(prefix, r.in2[s, j])
            if j < GROUP - 1:
                r.qpre[j + 1] = prefix
        r.qtot[s] = prefix

        @pl.when(spreads)
        def _():
            r.s4_out[s] = half(prefix[extent:])
            for k in range(2):
                spread_copy(s, k).start()

        mine = r.qpre[zl]
        mine_h = half(mine)
        comps = [mine]
        for j in range(1, GROUP):
            g = r.gpre[s, j - 1]
            comps.append(mine + dot(mine_h, half(g[0:extent])) + g)

        @pl.when(lower_quad)
        def _():
            give_states(s, [m[extent:] for m in comps])

        @pl.when(jnp.logical_not(lower_quad))
        def _():
            for j in range(GROUP):
                r.comp_d[s, j] = half(comps[j][0:extent])
                r.comp_c[s, j] = comps[j][extent:]

    tails = jnp.logical_or(z == GROUP, z == 2 * GROUP - 1)

    def tail_z(i):
        return jnp.where(z == GROUP, 2 + i, lax.rem(6 + i, 2 * GROUP))

    def tail_copy(s, i, xx):
        return pltpu.make_async_remote_copy(
            src_ref=r.tail_out.at[s, i * GROUP + xx], dst_ref=r.tail_in.at[s, x],
            send_sem=r.send_t.at[s, i * GROUP + xx], recv_sem=r.recv_t.at[s, x],
            device_id=sp_id(tail_z(i), xx), device_id_type=MESH,
        )

    def tail_self(i, xx):
        return jnp.logical_and(tail_z(i) == z, x == xx)

    def tail(s, s4, s4h):
        tot = r.qtot[s]
        memory = half(s4 + dot(s4h, half(tot[0:extent])) + tot[extent:]).astype(f32)
        shape = r.nq.shape
        mine = (iota(shape, 0) == s) & (iota(shape, 1) == x // 2)

        def own(ref):
            kept = jnp.where(mine, ref[...].astype(f32), 0.0)
            return jnp.sum(jnp.sum(kept, axis=0), axis=0, keepdims=True)

        qn, kn = unit_rows(own(r.nq)), unit_rows(own(r.nk))
        both = jnp.concatenate(
            [jnp.broadcast_to(qn, (PAD, extent)), jnp.broadcast_to(kn, (PAD, extent))], axis=0
        )
        twice = jnp.concatenate([memory, memory], axis=0)
        reads = dot(both, twice, NT, highest)
        recall, retrieve = reads[0:1], reads[PAD : PAD + 1]
        beta_new, decay_new = r.nb[s, x // 2], r.nd[s, x // 2]
        fresh = own(r.nv) - decay_new * retrieve
        meet = jnp.sum(kn * qn, axis=-1, keepdims=True)
        kept = (iota((1, extent), 1) // hv) == lax.rem(x, 2)
        read = jnp.where(kept, decay_new * recall + (beta_new * meet) * fresh, 0.0)
        r.memt[...] = jnp.where(kept, twice.T, 0.0)
        answer = jnp.broadcast_to(read, (4, extent))
        for i in range(GROUP):
            base = pl.multiple_of(tail_z(i) * 16, 16)
            keys = r.memt[pl.ds(base, 16), :]
            for xx in range(GROUP):
                r.tail_out[s, i * GROUP + xx, 0:4] = keys[xx * 4 : xx * 4 + 4]
                r.tail_out[s, i * GROUP + xx, 4:8] = answer
        for i in range(GROUP):
            for xx in range(GROUP):

                @pl.when(tail_self(i, xx))
                def _():
                    r.tail_in[s, x] = r.tail_out[s, i * GROUP + xx]

                @pl.when(jnp.logical_not(tail_self(i, xx)))
                def _():
                    tail_copy(s, i, xx).start()

    def upper(s):
        @pl.when(jnp.logical_not(lower_quad))
        def _():
            pltpu.make_async_remote_copy(
                src_ref=r.s4_out.at[s], dst_ref=r.s4_in.at[s], send_sem=r.send3.at[s, 0],
                recv_sem=r.recv3.at[s], device_id=sp_id(spread_from, x), device_id_type=MESH,
            ).wait_recv()
            s4h = r.s4_in[s]
            s4 = s4h.astype(f32)
            give_states(s, [s4 + dot(s4h, r.comp_d[s, j]) + r.comp_c[s, j] for j in range(GROUP)])

            @pl.when(tails)
            def _():
                tail(s, s4, s4h)

    def finish(s):
        for o in range(GROUP):

            @pl.when(x != o)
            def _():
                pltpu.make_async_remote_copy(
                    src_ref=r.st_out.at[s, 0], dst_ref=r.st_in.at[s, o], send_sem=r.send4.at[s, 0],
                    recv_sem=r.recv4.at[s, o], device_id=sp_id(z, o), device_id_type=MESH,
                ).wait_recv()

        for h in range(heads):
            state_t = jnp.concatenate([r.st_in[s, 2 * h], r.st_in[s, 2 * h + 1]], axis=0)
            o = r.local_out[s, h] + dot(r.reach[s, h], state_t, NT)
            norm = lax.rsqrt(jnp.mean(o * o, axis=-1, keepdims=True) + norm_floor)
            r.mixed[s, :, h * extent : (h + 1) * extent] = half(o * norm * r.gated[s, h])

    def last_read(s):
        from_z = jnp.where((z >= 2) & (z < 6), GROUP, 2 * GROUP - 1)
        for o in range(GROUP):

            @pl.when(jnp.logical_not((z == from_z) & (x == o)))
            def _():
                pltpu.make_async_remote_copy(
                    src_ref=r.tail_out.at[s, 0], dst_ref=r.tail_in.at[s, o], send_sem=r.send_t.at[s, 0],
                    recv_sem=r.recv_t.at[s, o], device_id=sp_id(from_z, o), device_id_type=MESH,
                ).wait_recv()

        for h in range(heads):
            both = r.tail_in[s, 2 * h] + r.tail_in[s, 2 * h + 1]
            r.cache[s, h] = half(both[0:4])
            read = both[4:5]
            norm = lax.rsqrt(jnp.mean(read * read, axis=-1, keepdims=True) + norm_floor)
            r.first[s : s + 1, h * extent : (h + 1) * extent] = read * norm * r.gain[...]

    start_own(0)
    near(0)
    first_arrivals(0)
    start_own(1)
    use(0, [(2, 0), (4, 1)])
    rest(0)
    local(0, lambda: first_arrivals(1))
    near(1)
    use(1, [(2, 0), (4, 1)])
    rest(1)
    local(1, lambda: None)
    combine_group(0)
    combine_group(1)
    combine_quad(0)
    upper(0)
    finish(0)
    combine_quad(1)
    upper(1)
    finish(1)
    last_read(0)
    last_read(1)

    for s in range(seqs):
        for copy in own_sends(s):
            copy.wait_send()
        for i in range(2):
            forward(s, i).wait_send()
        for i in range(3):
            for hf in range(2):
                partner_send(s, i, hf).wait_send()
        for o in range(GROUP):

            @pl.when(x != o)
            def _():
                x_copy(s, o).wait_send()
                state_copy(s, o).wait_send()

        for d in range(1, GROUP):
            quad_copy(s, d).wait_send()

        @pl.when(spreads)
        def _():
            for k in range(2):
                spread_copy(s, k).wait_send()

        @pl.when(tails)
        def _():
            for i in range(GROUP):
                for xx in range(GROUP):

                    @pl.when(jnp.logical_not(tail_self(i, xx)))
                    def _():
                        tail_copy(s, i, xx).wait_send()


def shards(
    tokens, query_weight, key_weight, value_weight, gate_weight, beta_weight, decay_weight,
    beta_bias, rate_log, out_gain, new_query, new_key, new_value, new_beta, new_decay,
):
    seqs, span, kd = tokens.shape
    heads = rate_log.shape[0]
    extent = out_gain.shape[0]
    depth, width = query_weight.shape
    kc = kd // 2
    hv, box = extent // 2, extent + extent // 2
    key_rows = extent // lax.axis_size("sp")
    vmem = pl.BlockSpec(memory_space=pltpu.VMEM)
    smem = pl.BlockSpec(memory_space=pltpu.SMEM)
    hbm = pl.BlockSpec(memory_space=pl.ANY)
    inputs = dict(
        x=hbm, wq=hbm, wk=hbm, wv=hbm, wg=hbm, bw=vmem, dw=vmem, bias=smem, rate=smem, gain=vmem,
        nq=vmem, nk=vmem, nv=vmem, nb=smem, nd=smem,
    )
    outputs = dict(
        mixed=jax.ShapeDtypeStruct((seqs, span, width), bf16),
        cache=jax.ShapeDtypeStruct((seqs, heads, key_rows, extent), bf16),
        first=jax.ShapeDtypeStruct((seqs, width), f32),
    )
    dma = pltpu.SemaphoreType.DMA
    scratch = dict(
        bd=pltpu.VMEM((2 * PAD, depth), bf16),
        xs=pltpu.VMEM((8, seqs, 2, span, kc), bf16),
        wbuf=pltpu.VMEM((4, 8, kd, width), bf16),
        acc=pltpu.VMEM((4, span, width), f32),
        sacc=pltpu.VMEM((2 * PAD, span), f32),
        rows=pltpu.VMEM((seqs, 4, span, width), bf16),
        local_out=pltpu.VMEM((seqs, heads, span, extent), f32),
        reach=pltpu.VMEM((seqs, heads, span, extent), bf16),
        gated=pltpu.VMEM((seqs, heads, span, extent), f32),
        out1=pltpu.VMEM((seqs, GROUP, box, extent), bf16),
        in1=pltpu.VMEM((seqs, GROUP, box, extent), bf16),
        gpre=pltpu.VMEM((seqs, GROUP - 1, box, extent), f32),
        in2=pltpu.VMEM((seqs, GROUP, box, extent), bf16),
        qpre=pltpu.VMEM((GROUP, box, extent), f32),
        qtot=pltpu.VMEM((seqs, box, extent), f32),
        comp_d=pltpu.VMEM((seqs, GROUP, extent, extent), bf16),
        comp_c=pltpu.VMEM((seqs, GROUP, hv, extent), f32),
        s4_out=pltpu.VMEM((seqs, hv, extent), bf16),
        s4_in=pltpu.VMEM((seqs, hv, extent), bf16),
        st_out=pltpu.VMEM((seqs, GROUP, hv, extent), bf16),
        st_in=pltpu.VMEM((seqs, GROUP, hv, extent), bf16),
        memt=pltpu.VMEM((extent, extent), f32),
        tail_out=pltpu.VMEM((seqs, GROUP * GROUP, PAD, extent), f32),
        tail_in=pltpu.VMEM((seqs, GROUP, PAD, extent), f32),
        tok_sem=dma((seqs, 2)),
        wsem=dma((4, 8)),
        own_sem=dma((2, seqs, 2)),
        fwd_sem=dma((2, seqs)),
        part_sem=dma((4, seqs, 2)),
        rx=dma((8, seqs, 2)),
        send1=dma((seqs, GROUP)),
        recv1=dma((seqs, GROUP)),
        send2=dma((seqs, GROUP)),
        recv2=dma((seqs, GROUP)),
        send3=dma((seqs, 2)),
        recv3=dma((seqs,)),
        send4=dma((seqs, GROUP)),
        recv4=dma((seqs, GROUP)),
        send_t=dma((seqs, GROUP * GROUP)),
        recv_t=dma((seqs, GROUP)),
    )
    names = list(inputs) + list(outputs) + list(scratch)
    dims = (seqs, heads, span, extent, kc)

    def body(*refs):
        fused_kernel(names, dims, *refs)

    return pl.pallas_call(
        body,
        out_shape=tuple(outputs.values()),
        in_specs=list(inputs.values()),
        out_specs=(vmem,) * 3,
        scratch_shapes=list(scratch.values()),
        compiler_params=pltpu.CompilerParams(
            collective_id=0, has_side_effects=True, vmem_limit_bytes=60 * 1024 * 1024
        ),
        name="fused",
    )(
        tokens, query_weight, key_weight, value_weight, gate_weight, beta_weight.T, decay_weight.T,
        beta_bias, rate_log, out_gain[None], new_query, new_key, new_value, new_beta, new_decay,
    )


def solution(mesh):
    placed = (
        P(None, "sp", "tp"),
        P(None, "tp"),
        P(None, "tp"),
        P(None, "tp"),
        P(None, "tp"),
        P(None, "tp"),
        P(None, "tp"),
        P("tp"),
        P("tp"),
        P(),
        P(None, "tp", None),
        P(None, "tp", None),
        P(None, "tp", None),
        P(None, "tp"),
        P(None, "tp"),
    )
    return jax.shard_map(
        shards,
        mesh=mesh,
        in_specs=placed,
        out_specs=(P(None, "sp", "tp"), P(None, "tp", "sp", None), P(None, "tp")),
        check_vma=False,
    )
```

time: 90.5 us -> 59.3 us (0.66)
  Pallas kernels: 84.8 us -> 53.8 us
    pallas_call x2 -> x1, Pallas kernels: 84.8 us -> 53.8 us  [shards(): pl.pallas_call(body, out_shape=tuple(outputs.values()), in_specs=list(inp...]
    unnamed x22 -> x3, local copies, waits for them, and re-layouts: 3.19 us -> 4.11 us
where the time goes in v1:
time: 59.3 us; the launch traced here: 58.5 us
  Pallas kernels  53.8 us (91%)
  local copies, waits for them, and re-layouts  4.11 us (7%)
  between operations  0.65 us (1%)
    pallas_call x1, Pallas kernels, shards(): pl.pallas_call(body, out_shape=tuple(outputs.values()), in_specs=list(inp...  53.8 us
    unnamed x3, local copies, waits for them, and re-layouts  4.11 us

profile of v1, /device:TPU:1, one launch (start us, length us, event | category | flops | bytes accessed | tf_op | source)
XLA Modules:
  0.0 58.5 jit_solution(17816162921976622464)
XLA Ops:
  0.6 53.8 %fused.1 = (bf16[2,192,256]{2,1,0:T(8,128)(2,1)}, bf16[2,2,4,128]{3,2,1,0:T(4,128)(2,1)}, f32[2,256]{1,0:T(2,128)}) custom-call(bf16[2,192,512]{2,1,0:T(8,128)(2,1)} %refs_0_.1, bf16[4096,256]{1,0:T(8,128)(2,1)} %refs_1_.1, bf16[4096,256]{1,0:T(8,128)(2,1)} %refs_2_.1, bf16[4096,256]{1,0:T(8,128)(2,1)} %refs_3_.1, bf16[4096,256]{1,0:T(8,128)(2,1)} %refs_4_.1, ...), custom_call_target="tpu_custom_call" | custom-call | tf_op jit(solution)/shard_map/fused/pallas_call | solution.py:653
  54.4 1.6 %copy.21 = bf16[2,192,256]{2,1,0:T(8,128)(2,1)} copy(bf16[2,192,256]{2,1,0:T(8,128)(2,1)} %get-tuple-element.6) | data formatting | bytes 393216
  56.0 1.3 %copy.22 = bf16[2,2,4,128]{3,2,1,0:T(4,128)(2,1)} copy(bf16[2,2,4,128]{3,2,1,0:T(4,128)(2,1)} %get-tuple-element.7) | data formatting | bytes 8192
  57.3 1.2 %copy.23 = f32[2,256]{1,0:T(2,128)} copy(f32[2,256]{1,0:T(2,128)} %get-tuple-element.8) | data formatting | bytes 4096

commit v2 on v1

--- a/solution.py
+++ b/solution.py
@@ -14,6 +14,7 @@
 PAD = 8
 GROUP = 4
 BLOCK = 64
+SMALL = ("bw", "dw", "bias", "rate", "gain", "nq", "nk", "nv", "nb", "nd")
 f32 = jnp.float32
 bf16 = jnp.bfloat16
 
@@ -83,22 +84,20 @@
     def peer_x(d):
         return lax.rem(x + d, GROUP)
 
-    def peer_zl(d):
-        return lax.rem(zl + d, GROUP)
-
-    def peer_z(d):
-        return z - zl + peer_zl(d)
-
     barrier = pltpu.get_barrier_semaphore()
 
     def greet(device):
         pl.semaphore_signal(barrier, inc=1, device_id=device, device_id_type=MESH)
 
-    for t in (nxt, prv, partner):
-        greet({"tp": t})
-    for d in range(1, GROUP):
-        greet(sp_id(z, peer_x(d)))
-        greet(sp_id(peer_z(d), x))
+    x_near = [sp_id(z, peer_x(d)) for d in (1, 3)]
+    z_near = [sp_id(lax.rem(z + d, 2 * GROUP), x) for d in (1, 2 * GROUP - 1)]
+    near_ones = [{"tp": t} for t in (nxt, prv, partner)] + x_near + z_near
+    for device in near_ones:
+        greet(device)
+
+    def relay(devices, sem):
+        for device in devices:
+            pl.semaphore_signal(sem, inc=1, device_id=device, device_id_type=MESH)
 
     is_a, is_b = z == GROUP - 1, z == 0
     spreads = jnp.logical_or(is_a, is_b)
@@ -106,20 +105,14 @@
     def spread_to(k):
         return jnp.where(is_a, GROUP + k, 2 * GROUP - 1 - k)
 
-    @pl.when(spreads)
-    def _():
-        for k in range(2):
-            greet(sp_id(spread_to(k), x))
-
     spread_from = jnp.where(z < GROUP + 2, GROUP - 1, 0)
 
-    @pl.when(jnp.logical_not(lower_quad))
-    def _():
-        greet(sp_id(spread_from, x))
+    def rows_of(s):
+        return pl.ds(s * span, span)
 
     def token_copy(s, hf):
         return pltpu.make_async_copy(
-            r.x.at[s, :, pl.ds(hf * kc, kc)], r.xs.at[me, s, hf], r.tok_sem.at[s, hf]
+            r.x.at[s, :, pl.ds(hf * kc, kc)], r.xs.at[me, hf, rows_of(s)], r.tok_sem.at[s, hf]
         )
 
     for s in range(seqs):
@@ -130,30 +123,35 @@
         start = pl.multiple_of(order[slot] * kd, kd)
         return pltpu.make_async_copy(weights[w].at[pl.ds(start, kd), :], r.wbuf.at[w, slot], r.wsem.at[w, slot])
 
+    def small_copy(name):
+        return pltpu.make_async_copy(
+            getattr(r, name + "_hbm"), getattr(r, name), r.small_sem.at[SMALL.index(name)]
+        )
+
     for slot in range(8):
         for w in range(4):
             weight_copy(w, slot).start()
+    for name in SMALL:
+        small_copy(name).start()
     r.bd[...] = jnp.zeros_like(r.bd)
-    r.bd[0:heads] = r.bw[...]
-    r.bd[PAD : PAD + heads] = r.dw[...]
-    extra = jnp.where(spreads, 2, jnp.where(lower_quad, 0, 1))
-    pl.semaphore_wait(barrier, 3 + 2 * (GROUP - 1) + extra)
+    pl.semaphore_wait(barrier, len(near_ones))
 
     def ring(b, s, hf, to, sem):
         return pltpu.make_async_remote_copy(
-            src_ref=r.xs.at[b, s, hf], dst_ref=r.xs.at[b, s, hf], send_sem=sem,
+            src_ref=r.xs.at[b, hf, rows_of(s)], dst_ref=r.xs.at[b, hf, rows_of(s)], send_sem=sem,
             recv_sem=r.rx.at[b, s, hf], device_id={"tp": to}, device_id_type=MESH,
         )
 
-    def own_sends(s):
-        return [
-            ring(me, s, 0, nxt, r.own_sem.at[0, s, 0]),
-            ring(me, s, 1, prv, r.own_sem.at[1, s, 1]),
-            ring(me, s, 1, nxt, r.own_sem.at[0, s, 1]),
-            ring(me, s, 0, prv, r.own_sem.at[1, s, 0]),
-            ring(me, s, 0, partner, r.part_sem.at[0, s, 0]),
-            ring(me, s, 1, partner, r.part_sem.at[0, s, 1]),
-        ]
+    def own_send(s, i, step):
+        hf = i if step == 0 else 1 - i
+        return ring(me, s, hf, (nxt, prv)[i], r.own_sem.at[i, s, hf])
+
+    def own_partner(s, hf):
+        return ring(me, s, hf, partner, r.part_sem.at[0, s, hf])
+
+    def start_own(s, step):
+        for i in range(2):
+            own_send(s, i, step).start()
 
     def forward(s, i):
         return ring((prv, nxt)[i], s, i, (nxt, prv)[i], r.fwd_sem.at[i, s])
@@ -164,78 +162,93 @@
     def arrive(b, s, hf):
         ring(b, s, hf, partner, r.part_sem.at[0, s, hf]).wait_recv()
 
-    def use(s, items, first=False):
-        parts = [r.xs[order[slot], s, hf] for slot, hf in items]
-        if s == 0:
-            for slot in sorted({slot for slot, hf in items} - set(waited)):
-                waited.append(slot)
-                for w in range(4):
-                    weight_copy(w, slot).wait()
+    def use(seq_list, items, first=False):
+        at = pl.ds(seq_list[0] * span, len(seq_list) * span)
+        parts = [r.xs[order[slot], hf, at] for slot, hf in items]
+        for slot in sorted({slot for slot, hf in items} - set(waited)):
+            waited.append(slot)
+            for w in range(4):
+                weight_copy(w, slot).wait()
         for w in range(4):
             total = None
             for (slot, hf), part in zip(items, parts):
                 term = dot(part, r.wbuf[w, slot, hf * kc : (hf + 1) * kc, :])
                 total = term if total is None else total + term
-            r.acc[w] = total if first else r.acc[w] + total
-        total = None
-        for (slot, hf), part in zip(items, parts):
-            piece = r.bd[:, pl.ds(pl.multiple_of(order[slot] * kd + hf * kc, kc), kc)]
-            term = dot(piece, part, NT)
-            total = term if total is None else total + term
-        r.sacc[...] = total if first else r.sacc[...] + total
+            r.acc[w, at] = total if first else r.acc[w, at] + total
+        for i, s in enumerate(seq_list):
+            total = None
+            for (slot, hf), part in zip(items, parts):
+                piece = r.bd[:, pl.ds(pl.multiple_of(order[slot] * kd + hf * kc, kc), kc)]
+                term = dot(piece, part[i * span : (i + 1) * span], NT)
+                total = term if total is None else total + term
+            r.sacc[s] = total if first else r.sacc[s] + total
 
     waited = []
-
-    def start_own(s):
+    both = list(range(seqs))
+
+    def begin():
         for hf in range(2):
-            token_copy(s, hf).wait()
-        for copy in own_sends(s):
-            copy.start()
-
-    def first_arrivals(s):
+            token_copy(0, hf).wait()
+        for step in range(2):
+            start_own(0, step)
+        for hf in range(2):
+            own_partner(0, hf).start()
+        for s in range(1, seqs):
+            for hf in range(2):
+                token_copy(s, hf).wait()
+                own_partner(s, hf).start()
+        relay(x_near, r.relay_x)
+        relay(z_near, r.relay_z.at[0])
+        for name in SMALL:
+            small_copy(name).wait()
+        r.bd[0:heads] = r.bw[...]
+        r.bd[PAD : PAD + heads] = r.dw[...]
+
+    def near():
+        use(both, [(0, 0), (0, 1)], True)
+        for s in both:
+            for hf in range(2):
+                arrive(partner, s, hf)
+        use(both, [(1, 0), (1, 1)])
+        pl.semaphore_wait(r.relay_x, 2)
+        pl.semaphore_wait(r.relay_z.at[0], 2)
+        relay(z_near, r.relay_z.at[1])
+
+    def near_first(s):
         arrive(prv, s, 0)
         forward(s, 0).start()
+        partner_send(s, 0, 0).start()
         arrive(nxt, s, 1)
         forward(s, 1).start()
-        partner_send(s, 0, 0).start()
         partner_send(s, 1, 1).start()
 
-    def rest(s):
-        arrive(order[3], s, 0)
-        arrive(order[5], s, 1)
-        use(s, [(3, 0), (5, 1)])
+    def near_second(s):
         arrive(prv, s, 1)
         partner_send(s, 0, 1).start()
         arrive(nxt, s, 0)
         partner_send(s, 1, 0).start()
-        use(s, [(2, 1), (4, 0)])
+
+    def far(s):
+        for hf in range(2):
+            arrive(opp, s, hf)
+            partner_send(s, 2, hf).start()
+
+    def cross_first(s):
+        arrive(order[3], s, 0)
+        arrive(order[5], s, 1)
+
+    def cross_second(s):
         arrive(order[3], s, 1)
         arrive(order[5], s, 0)
-        use(s, [(3, 1), (5, 0)])
-        arrive(opp, s, 0)
-        partner_send(s, 2, 0).start()
-        arrive(opp, s, 1)
-        partner_send(s, 2, 1).start()
-        use(s, [(6, 0), (6, 1)])
-        arrive(order[7], s, 0)
-        arrive(order[7], s, 1)
-        use(s, [(7, 0), (7, 1)])
+
+    def cross_far(s):
+        for hf in range(2):
+            arrive(order[7], s, hf)
+
+    def round_rows(s):
         for w in range(4):
-            r.rows[s, w] = half(r.acc[w])
-
-    def near(s):
-        use(s, [(0, 0), (0, 1)], True)
-        for hf in range(2):
-            arrive(partner, s, hf)
-        use(s, [(1, 0), (1, 1)])
-
-
-    slot_of = iota((PAD, 1), 0)
-    bias = jnp.zeros((PAD, 1), f32)
-    rate = jnp.zeros((PAD, 1), f32)
-    for h in range(heads):
-        bias = jnp.where(slot_of == h, r.bias[h], bias)
-        rate = jnp.where(slot_of == h, r.rate[h], rate)
+            r.rows[s, w] = half(r.acc[w, rows_of(s)])
+
 
     def x_copy(s, o):
         return pltpu.make_async_remote_copy(
@@ -243,10 +256,16 @@
             recv_sem=r.recv1.at[s, x], device_id=sp_id(z, o), device_id_type=MESH,
         )
 
-    def local(s, hook):
+    def local(s, hook, hook2):
+        slot_of = iota((PAD, 1), 0)
+        bias = jnp.zeros((PAD, 1), f32)
+        rate = jnp.zeros((PAD, 1), f32)
+        for h in range(heads):
+            bias = jnp.where(slot_of == h, r.bias[h], bias)
+            rate = jnp.where(slot_of == h, r.rate[h], rate)
         upper = jnp.where(iota((span, span), 0) <= iota((span, span), 1), 1.0, 0.0)
-        beta8 = jax.nn.sigmoid(r.sacc[0:PAD] + bias)
-        pre = r.sacc[PAD : 2 * PAD]
+        beta8 = jax.nn.sigmoid(r.sacc[s, 0:PAD] + bias)
+        pre = r.sacc[s, PAD : 2 * PAD]
         soft = jnp.maximum(pre, 0.0) + jnp.log1p(jnp.exp(-jnp.abs(pre)))
         cum8 = dot(-jnp.exp(rate) * soft, upper, NN, highest)
         cum_t, beta_t = cum8.T, beta8.T
@@ -284,6 +303,7 @@
             )
         hook()
         inv = unit_lower_inverses(diags)
+        hook2()
         done = [[] for _ in range(heads)]
         for i in range(nblk):
             at = slice(i * BLOCK, (i + 1) * BLOCK)
@@ -303,15 +323,9 @@
             for f in range(2):
                 r.out1[s, 2 * h + f, 0:extent, :] = step
                 r.out1[s, 2 * h + f, extent:, :] = state[f * hv : (f + 1) * hv]
-        for o in range(GROUP):
-
-            @pl.when(x != o)
-            def _():
-                x_copy(s, o).start()
-
-            @pl.when(x == o)
-            def _():
-                r.in1[s, x] = r.out1[s, o]
+        for d in (2, 1, 3):
+            x_copy(s, peer_x(d)).start()
+        r.in1[s, x] = r.out1[s, x]
 
         for h in range(heads):
             e = per_head[h]
@@ -330,11 +344,47 @@
         e = step[0:extent]
         return prefix + dot(half(prefix), e) + step.astype(f32)
 
-    def quad_copy(s, d):
+    def quad_copy(s, j, source, part):
         return pltpu.make_async_remote_copy(
-            src_ref=r.in2.at[s, zl], dst_ref=r.in2.at[s, zl], send_sem=r.send2.at[s, d - 1],
-            recv_sem=r.recv2.at[s, zl], device_id=sp_id(peer_z(d), x), device_id_type=MESH,
+            src_ref=r.in2.at[s, source, part], dst_ref=r.in2.at[s, source, part],
+            send_sem=r.send2.at[s, j], recv_sem=r.recv2.at[s, source],
+            device_id=sp_id(z - zl + j, x), device_id_type=MESH,
         )
+
+    whole, state_only = pl.ds(0, box), pl.ds(extent, hv)
+
+    def quad_each(s, act):
+        for j in (3, 2, 1, 0):
+            if j:
+
+                @pl.when(is_b)
+                def _():
+                    act(quad_copy(s, j, zl, state_only))
+
+                @pl.when(jnp.logical_and(zl < j, jnp.logical_not(is_b)))
+                def _():
+                    act(quad_copy(s, j, zl, whole))
+            else:
+
+                @pl.when(zl > 0)
+                def _():
+                    act(quad_copy(s, 0, zl, whole))
+
+    def quad_arrive(s, j):
+        if j == 0:
+
+            @pl.when(jnp.logical_and(zl > 0, lower_quad))
+            def _():
+                quad_copy(s, 0, 0, state_only).wait_recv()
+
+            @pl.when(jnp.logical_and(zl > 0, jnp.logical_not(lower_quad)))
+            def _():
+                quad_copy(s, 0, 0, whole).wait_recv()
+        else:
+
+            @pl.when(jnp.logical_or(zl > j, zl == 0))
+            def _():
+                quad_copy(s, 0, j, whole).wait_recv()
 
     def combine_group(s):
         for j in range(GROUP):
@@ -351,8 +401,7 @@
             r.gpre[s, j - 1] = prefix
             prefix = compose(prefix, r.in1[s, j])
         r.in2[s, zl] = half(prefix)
-        for d in (3, 2, 1):
-            quad_copy(s, d).start()
+        quad_each(s, lambda copy: copy.start())
 
     def spread_copy(s, k):
         return pltpu.make_async_remote_copy(
@@ -369,54 +418,79 @@
     def give_states(s, states):
         for xx in range(GROUP):
             r.st_out[s, xx] = half(states[xx])
-        for xx in range(GROUP):
-
-            @pl.when(x != xx)
-            def _():
-                state_copy(s, xx).start()
-
-            @pl.when(x == xx)
-            def _():
-                r.st_in[s, x] = r.st_out[s, xx]
-
-    def combine_quad(s):
-        for d in range(1, GROUP):
-            j = peer_zl(d)
-            pltpu.make_async_remote_copy(
-                src_ref=r.in2.at[s, j], dst_ref=r.in2.at[s, j], send_sem=r.send2.at[s, 0],
-                recv_sem=r.recv2.at[s, j], device_id=sp_id(peer_z(d), x), device_id_type=MESH,
-            ).wait_recv()
-        r.qpre[0] = jnp.zeros((box, extent), f32)
-        prefix = r.in2[s, 0].astype(f32)
-        r.qpre[1] = prefix
-        for j in range(1, GROUP):
-            prefix = compose(prefix, r.in2[s, j])
-            if j < GROUP - 1:
-                r.qpre[j + 1] = prefix
-        r.qtot[s] = prefix
-
-        @pl.when(spreads)
-        def _():
-            r.s4_out[s] = half(prefix[extent:])
-            for k in range(2):
-                spread_copy(s, k).start()
-
-        mine = r.qpre[zl]
-        mine_h = half(mine)
+        for d in (2, 1, 3):
+            state_copy(s, peer_x(d)).start()
+        r.st_in[s, x] = r.st_out[s, x]
+
+    def with_groups(mine, mine_h, take, s):
         comps = [mine]
         for j in range(1, GROUP):
             g = r.gpre[s, j - 1]
-            comps.append(mine + dot(mine_h, half(g[0:extent])) + g)
-
+            comps.append(mine + dot(mine_h, half(g[0:extent])) + g[take])
+        return comps
+
+    def combine_lower(s):
+        r.qs[0] = jnp.zeros((hv, extent), f32)
+
+        def give():
+            mine = r.qs[zl]
+            give_states(s, with_groups(mine, half(mine), slice(extent, box), s))
+
+        @pl.when(is_b)
+        def _():
+            give()
+
+        for j in range(GROUP):
+
+            @pl.when(jnp.logical_or(zl > j, spreads))
+            def _():
+                quad_arrive(s, j)
+                step = r.in2[s, j, extent:].astype(f32)
+                if j:
+                    state = r.qs[j]
+                    step = state + dot(half(state), r.in2[s, j, 0:extent]) + step
+                r.qs[j + 1] = step
+
+        @pl.when(spreads)
+        def _():
+            r.s4_out[s] = half(r.qs[GROUP])
+            for k in range(2):
+                spread_copy(s, k).start()
+
+        @pl.when(jnp.logical_not(is_b))
+        def _():
+            give()
+
+    ends = jnp.logical_or(zl == 0, zl == GROUP - 1)
+
+    def combine_upper(s):
+        r.qpre[0] = jnp.zeros((box, extent), f32)
+        for j in range(GROUP):
+
+            @pl.when(jnp.logical_or(zl > j, ends))
+            def _():
+                quad_arrive(s, j)
+                got = r.in2[s, j]
+                r.qpre[j + 1] = got.astype(f32) if j == 0 else compose(r.qpre[j], got)
+
+        @pl.when(ends)
+        def _():
+            r.qtot[s] = r.qpre[GROUP]
+
+        mine = r.qpre[zl]
+        comps = with_groups(mine, half(mine), slice(0, box), s)
+        for j in range(GROUP):
+            r.comp_d[s, j] = half(comps[j][0:extent])
+            r.comp_c[s, j] = comps[j][extent:]
+
+    def combine_quad(s):
         @pl.when(lower_quad)
         def _():
-            give_states(s, [m[extent:] for m in comps])
+            combine_lower(s)
 
         @pl.when(jnp.logical_not(lower_quad))
         def _():
-            for j in range(GROUP):
-                r.comp_d[s, j] = half(comps[j][0:extent])
-                r.comp_c[s, j] = comps[j][extent:]
+            combine_upper(s)
 
     tails = jnp.logical_or(z == GROUP, z == 2 * GROUP - 1)
 
@@ -433,29 +507,31 @@
     def tail_self(i, xx):
         return jnp.logical_and(tail_z(i) == z, x == xx)
 
+    def prepare_read(s):
+        shape = r.nq.shape
+        mine = (iota(shape, 0) == s) & (iota(shape, 1) == x // 2)
+
+        def own(ref):
+            kept = jnp.where(mine, ref[...].astype(f32), 0.0)
+            return jnp.sum(jnp.sum(kept, axis=0), axis=0, keepdims=True)
+
+        qn, kn = unit_rows(own(r.nq)), unit_rows(own(r.nk))
+        r.pair_row[s, 0:1] = own(r.nv)
+        r.pair_row[s, 1:2] = jnp.broadcast_to(jnp.sum(kn * qn, axis=-1, keepdims=True), (1, extent))
+        for i, row in enumerate((qn, kn)):
+            r.pair_col[s, i] = jnp.broadcast_to(row, (extent, extent)).T
+
     def tail(s, s4, s4h):
         tot = r.qtot[s]
         memory = half(s4 + dot(s4h, half(tot[0:extent])) + tot[extent:]).astype(f32)
-        shape = r.nq.shape
-        mine = (iota(shape, 0) == s) & (iota(shape, 1) == x // 2)
-
-        def own(ref):
-            kept = jnp.where(mine, ref[...].astype(f32), 0.0)
-            return jnp.sum(jnp.sum(kept, axis=0), axis=0, keepdims=True)
-
-        qn, kn = unit_rows(own(r.nq)), unit_rows(own(r.nk))
-        both = jnp.concatenate(
-            [jnp.broadcast_to(qn, (PAD, extent)), jnp.broadcast_to(kn, (PAD, extent))], axis=0
-        )
-        twice = jnp.concatenate([memory, memory], axis=0)
-        reads = dot(both, twice, NT, highest)
-        recall, retrieve = reads[0:1], reads[PAD : PAD + 1]
+        twice = jnp.concatenate([memory, memory], axis=0).T
+        recall = jnp.sum(twice * r.pair_col[s, 0], axis=0, keepdims=True)
+        retrieve = jnp.sum(twice * r.pair_col[s, 1], axis=0, keepdims=True)
         beta_new, decay_new = r.nb[s, x // 2], r.nd[s, x // 2]
-        fresh = own(r.nv) - decay_new * retrieve
-        meet = jnp.sum(kn * qn, axis=-1, keepdims=True)
+        fresh = r.pair_row[s, 0:1] - decay_new * retrieve
         kept = (iota((1, extent), 1) // hv) == lax.rem(x, 2)
-        read = jnp.where(kept, decay_new * recall + (beta_new * meet) * fresh, 0.0)
-        r.memt[...] = jnp.where(kept, twice.T, 0.0)
+        read = jnp.where(kept, decay_new * recall + (beta_new * r.pair_row[s, 1:2]) * fresh, 0.0)
+        r.memt[...] = jnp.where(kept, twice, 0.0)
         answer = jnp.broadcast_to(read, (4, extent))
         for i in range(GROUP):
             base = pl.multiple_of(tail_z(i) * 16, 16)
@@ -523,45 +599,65 @@
             norm = lax.rsqrt(jnp.mean(read * read, axis=-1, keepdims=True) + norm_floor)
             r.first[s : s + 1, h * extent : (h + 1) * extent] = read * norm * r.gain[...]
 
-    start_own(0)
-    near(0)
-    first_arrivals(0)
-    start_own(1)
-    use(0, [(2, 0), (4, 1)])
-    rest(0)
-    local(0, lambda: first_arrivals(1))
-    near(1)
-    use(1, [(2, 0), (4, 1)])
-    rest(1)
-    local(1, lambda: None)
-    combine_group(0)
-    combine_group(1)
-    combine_quad(0)
-    upper(0)
-    finish(0)
-    combine_quad(1)
-    upper(1)
-    finish(1)
-    last_read(0)
-    last_read(1)
-
+    def phase(name, step, *args):
+        with jax.named_scope(name):
+            step(*args)
+
+    def group0_early():
+        pl.semaphore_wait(r.relay_z.at[1], 2)
+        phase("group0", combine_group, 0)
+
+    phase("begin", begin)
+    phase("near", near)
+    phase("nf0", near_first, 0)
+    phase("u0a", use, [0], [(2, 0), (4, 1)])
+    phase("ns0", near_second, 0)
+    phase("own1a", start_own, 1, 0)
+    phase("cf0", cross_first, 0)
+    phase("u0b", use, [0], [(3, 0), (5, 1), (2, 1), (4, 0)])
+    phase("far0", far, 0)
+    phase("own1b", start_own, 1, 1)
+    phase("cs0", cross_second, 0)
+    phase("u0c", use, [0], [(3, 1), (5, 0), (6, 0), (6, 1)])
+    phase("cfar0", cross_far, 0)
+    phase("u0d", use, [0], [(7, 0), (7, 1)])
+    phase("rows0", round_rows, 0)
+    phase("local0", local, 0, lambda: phase("nf1", near_first, 1), lambda: phase("ns1", near_second, 1))
+    phase("u1a", use, [1], [(2, 0), (4, 1), (2, 1), (4, 0)])
+    phase("far1", far, 1)
+    phase("cc1", cross_first, 1)
+    phase("cs1", cross_second, 1)
+    phase("u1b", use, [1], [(3, 0), (5, 1), (3, 1), (5, 0)])
+    phase("u1c", use, [1], [(6, 0), (6, 1)])
+    phase("cfar1", cross_far, 1)
+    phase("u1d", use, [1], [(7, 0), (7, 1)])
+    phase("rows1", round_rows, 1)
+    phase("local1", local, 1, group0_early, lambda: None)
     for s in range(seqs):
-        for copy in own_sends(s):
-            copy.wait_send()
+        phase(f"prep{s}", prepare_read, s)
+    phase("group1", combine_group, 1)
+    phase("quad0", combine_quad, 0)
+    phase("upper0", upper, 0)
+    phase("quad1", combine_quad, 1)
+    phase("finish0", finish, 0)
+    phase("upper1", upper, 1)
+    phase("finish1", finish, 1)
+    phase("read0", last_read, 0)
+    phase("read1", last_read, 1)
+
+    for s in range(seqs):
         for i in range(2):
+            own_partner(s, i).wait_send()
             forward(s, i).wait_send()
+            for step in range(2):
+                own_send(s, i, step).wait_send()
         for i in range(3):
             for hf in range(2):
                 partner_send(s, i, hf).wait_send()
-        for o in range(GROUP):
-
-            @pl.when(x != o)
-            def _():
-                x_copy(s, o).wait_send()
-                state_copy(s, o).wait_send()
-
         for d in range(1, GROUP):
-            quad_copy(s, d).wait_send()
+            x_copy(s, peer_x(d)).wait_send()
+            state_copy(s, peer_x(d)).wait_send()
+        quad_each(s, lambda copy: copy.wait_send())
 
         @pl.when(spreads)
         def _():
@@ -590,12 +686,8 @@
     hv, box = extent // 2, extent + extent // 2
     key_rows = extent // lax.axis_size("sp")
     vmem = pl.BlockSpec(memory_space=pltpu.VMEM)
-    smem = pl.BlockSpec(memory_space=pltpu.SMEM)
-    hbm = pl.BlockSpec(memory_space=pl.ANY)
-    inputs = dict(
-        x=hbm, wq=hbm, wk=hbm, wv=hbm, wg=hbm, bw=vmem, dw=vmem, bias=smem, rate=smem, gain=vmem,
-        nq=vmem, nk=vmem, nv=vmem, nb=smem, nd=smem,
-    )
+    hbm = pl.BlockSpec(memory_space=pltpu.HBM)
+    inputs = ["x", "wq", "wk", "wv", "wg"] + [n + "_hbm" for n in SMALL]
     outputs = dict(
         mixed=jax.ShapeDtypeStruct((seqs, span, width), bf16),
         cache=jax.ShapeDtypeStruct((seqs, heads, key_rows, extent), bf16),
@@ -603,11 +695,22 @@
     )
     dma = pltpu.SemaphoreType.DMA
     scratch = dict(
+        bw=pltpu.VMEM((heads, depth), bf16),
+        dw=pltpu.VMEM((heads, depth), bf16),
+        bias=pltpu.SMEM((heads,), f32),
+        rate=pltpu.SMEM((heads,), f32),
+        gain=pltpu.VMEM((1, extent), f32),
+        nq=pltpu.VMEM((seqs, heads, extent), bf16),
+        nk=pltpu.VMEM((seqs, heads, extent), bf16),
+        nv=pltpu.VMEM((seqs, heads, extent), bf16),
+        nb=pltpu.SMEM((seqs, heads), f32),
+        nd=pltpu.SMEM((seqs, heads), f32),
+        small_sem=dma((len(SMALL),)),
         bd=pltpu.VMEM((2 * PAD, depth), bf16),
-        xs=pltpu.VMEM((8, seqs, 2, span, kc), bf16),
+        xs=pltpu.VMEM((8, 2, seqs * span, kc), bf16),
         wbuf=pltpu.VMEM((4, 8, kd, width), bf16),
-        acc=pltpu.VMEM((4, span, width), f32),
-        sacc=pltpu.VMEM((2 * PAD, span), f32),
+        acc=pltpu.VMEM((4, seqs * span, width), f32),
+        sacc=pltpu.VMEM((seqs, 2 * PAD, span), f32),
         rows=pltpu.VMEM((seqs, 4, span, width), bf16),
         local_out=pltpu.VMEM((seqs, heads, span, extent), f32),
         reach=pltpu.VMEM((seqs, heads, span, extent), bf16),
@@ -616,7 +719,12 @@
         in1=pltpu.VMEM((seqs, GROUP, box, extent), bf16),
         gpre=pltpu.VMEM((seqs, GROUP - 1, box, extent), f32),
         in2=pltpu.VMEM((seqs, GROUP, box, extent), bf16),
-        qpre=pltpu.VMEM((GROUP, box, extent), f32),
+        qpre=pltpu.VMEM((GROUP + 1, box, extent), f32),
+        qs=pltpu.VMEM((GROUP + 1, hv, extent), f32),
+        pair_row=pltpu.VMEM((seqs, PAD, extent), f32),
+        pair_col=pltpu.VMEM((seqs, 2, extent, extent), f32),
+        relay_x=pltpu.SemaphoreType.REGULAR,
+        relay_z=pltpu.SemaphoreType.REGULAR((2,)),
         qtot=pltpu.VMEM((seqs, box, extent), f32),
         comp_d=pltpu.VMEM((seqs, GROUP, extent, extent), bf16),
         comp_c=pltpu.VMEM((seqs, GROUP, hv, extent), f32),
@@ -644,7 +752,7 @@
         send_t=dma((seqs, GROUP * GROUP)),
         recv_t=dma((seqs, GROUP)),
     )
-    names = list(inputs) + list(outputs) + list(scratch)
+    names = inputs + list(outputs) + list(scratch)
     dims = (seqs, heads, span, extent, kc)
 
     def body(*refs):
@@ -653,16 +761,21 @@
     return pl.pallas_call(
         body,
         out_shape=tuple(outputs.values()),
-        in_specs=list(inputs.values()),
+        in_specs=[hbm] * len(inputs),
         out_specs=(vmem,) * 3,
         scratch_shapes=list(scratch.values()),
         compiler_params=pltpu.CompilerParams(
-            collective_id=0, has_side_effects=True, vmem_limit_bytes=60 * 1024 * 1024
+            collective_id=0, has_side_effects=True, vmem_limit_bytes=32 * 1024 * 1024
         ),
         name="fused",
     )(
-        tokens, query_weight, key_weight, value_weight, gate_weight, beta_weight.T, decay_weight.T,
-        beta_bias, rate_log, out_gain[None], new_query, new_key, new_value, new_beta, new_decay,
+        *(
+            pltpu.with_memory_space_constraint(value, pltpu.HBM)
+            for value in (
+                tokens, query_weight, key_weight, value_weight, gate_weight, beta_weight.T, decay_weight.T,
+                beta_bias, rate_log, out_gain[None], new_query, new_key, new_value, new_beta, new_decay,
+            )
+        )
     )
 
 

time: 59.3 us -> 53.6 us (0.904)
  the two profiles are of different devices: /device:TPU:1 before, /device:TPU:32 now
where the time goes in v2:
time: 53.6 us
  Pallas kernels  51.1 us (95%)
  local copies, waits for them, and re-layouts  1.85 us (3%)
  between operations  0.65 us (1%)
    pallas_call x1, Pallas kernels, shards(): pl.pallas_call(body, out_shape=tuple(outputs.values()), in_specs=[hbm] *...  51.1 us
    unnamed x3, local copies, waits for them, and re-layouts  1.85 us

profile of v2, /device:TPU:32, one launch (start us, length us, event | category | flops | bytes accessed | tf_op | source)
XLA Modules:
  0.0 53.6 jit_solution(8588356577675206075)
XLA Ops:
  0.6 51.1 %fused.1 = (bf16[2,192,256]{2,1,0:T(8,128)(2,1)S(1)}, bf16[2,2,4,128]{3,2,1,0:T(4,128)(2,1)S(1)}, f32[2,256]{1,0:T(2,128)S(1)}) custom-call(bf16[2,192,512]{2,1,0:T(8,128)(2,1)} %refs_0_.1, bf16[4096,256]{1,0:T(8,128)(2,1)} %refs_1_.1, bf16[4096,256]{1,0:T(8,128)(2,1)} %refs_2_.1, bf16[4096,256]{1,0:T(8,128)(2,1)} %refs_3_.1, bf16[4096,256]{1,0:T(8,128)(2,1)} %refs_4_.1, ...), custom_call_target="tpu_custom_call" | custom-call | tf_op jit(solution)/shard_map/fused/pallas_call | solution.py:761
  51.7 0.7 %copy.21 = bf16[2,192,256]{2,1,0:T(8,128)(2,1)} copy(bf16[2,192,256]{2,1,0:T(8,128)(2,1)S(1)} %get-tuple-element.6) | data formatting | bytes 393216
  52.4 0.6 %copy.22 = bf16[2,2,4,128]{3,2,1,0:T(4,128)(2,1)} copy(bf16[2,2,4,128]{3,2,1,0:T(4,128)(2,1)S(1)} %get-tuple-element.7) | data formatting | bytes 8192
  53.0 0.6 %copy.23 = f32[2,256]{1,0:T(2,128)} copy(f32[2,256]{1,0:T(2,128)S(1)} %get-tuple-element.8) | data formatting | bytes 4096

commit v3 on v2

--- a/solution.py
+++ b/solution.py
@@ -43,15 +43,23 @@
     size = blocks[0].shape[0]
     row, col = iota((size, size), 0), iota((size, size), 1)
     unit = jnp.where(row == col, 1.0, 0.0)
-    pair = ((row >> 1) == (col >> 1)) & (row > col)
-    inv = [unit - jnp.where(pair, b, 0.0) for b in blocks]
-    level = 1
+    four = ((row >> 2) == (col >> 2)) & (row > col)
+    low = [jnp.where(four, b, 0.0) for b in blocks]
+    low_h = [half(g) for g in low]
+    square = [dot(g, g) for g in low_h]
+    inv = [unit - g + q - dot(half(q), gh) for g, gh, q in zip(low, low_h, square)]
+    level = 2
     while (1 << level) < size:
-        mask = ((row >> (level + 1)) == (col >> (level + 1))) & ((row >> level) > (col >> level))
-        inv_h = [half(m) for m in inv]
-        mid = [half(dot(half(jnp.where(mask, b, 0.0)), m)) for b, m in zip(blocks, inv_h)]
-        inv = [m - dot(mh, t) for m, mh, t in zip(inv, inv_h, mid)]
-        level += 1
+        mask = ((row >> (level + 2)) == (col >> (level + 2))) & ((row >> level) > (col >> level))
+        t = [half(m) for m in inv]
+        g = [dot(th, half(jnp.where(mask, b, 0.0))) for th, b in zip(t, blocks)]
+        gh = [half(m) for m in g]
+        first = [dot(m, th) for m, th in zip(gh, t)]
+        second = [dot(m, m) for m in gh]
+        inv = [
+            m - f + dot(half(gg - q), half(f)) for m, f, gg, q in zip(inv, first, g, second)
+        ]
+        level += 2
     return [half(m) for m in inv]
 
 
@@ -128,11 +136,11 @@
             getattr(r, name + "_hbm"), getattr(r, name), r.small_sem.at[SMALL.index(name)]
         )
 
+    for name in SMALL:
+        small_copy(name).start()
     for slot in range(8):
         for w in range(4):
             weight_copy(w, slot).start()
-    for name in SMALL:
-        small_copy(name).start()
     r.bd[...] = jnp.zeros_like(r.bd)
     pl.semaphore_wait(barrier, len(near_ones))
 
@@ -256,67 +264,75 @@
             recv_sem=r.recv1.at[s, x], device_id=sp_id(z, o), device_id_type=MESH,
         )
 
-    def local(s, hook, hook2):
+    def local(s, hook, after):
         slot_of = iota((PAD, 1), 0)
         bias = jnp.zeros((PAD, 1), f32)
         rate = jnp.zeros((PAD, 1), f32)
         for h in range(heads):
             bias = jnp.where(slot_of == h, r.bias[h], bias)
             rate = jnp.where(slot_of == h, r.rate[h], rate)
-        upper = jnp.where(iota((span, span), 0) <= iota((span, span), 1), 1.0, 0.0)
+        upper = half(jnp.where(iota((span, span), 0) <= iota((span, span), 1), 1.0, 0.0))
         beta8 = jax.nn.sigmoid(r.sacc[s, 0:PAD] + bias)
         pre = r.sacc[s, PAD : 2 * PAD]
         soft = jnp.maximum(pre, 0.0) + jnp.log1p(jnp.exp(-jnp.abs(pre)))
-        cum8 = dot(-jnp.exp(rate) * soft, upper, NN, highest)
+        decay = -jnp.exp(rate) * soft
+        high = half(decay).astype(f32)
+        mid = half(decay - high).astype(f32)
+        thirds = dot(half(jnp.concatenate([high, mid, decay - high - mid], axis=0)), upper)
+        cum8 = thirds[0:PAD] + thirds[PAD : 2 * PAD] + thirds[2 * PAD :]
         cum_t, beta_t = cum8.T, beta8.T
+        r.cum_row[s] = cum8
+        r.cum_col[s] = cum_t
         row, col = iota((BLOCK, BLOCK), 0), iota((BLOCK, BLOCK), 1)
         causal = row >= col
         per_head = []
         diags = []
         for h in range(heads):
             lanes = slice(h * extent, (h + 1) * extent)
-            q = unit_rows(r.rows[s, 0, :, lanes].astype(f32))
             k = unit_rows(r.rows[s, 1, :, lanes].astype(f32))
             v = r.rows[s, 2, :, lanes].astype(f32)
             cumc, beta = cum_t[:, h : h + 1], beta_t[:, h : h + 1]
             cumr = cum8[h : h + 1, :]
             kb = k * beta
-            qh, kh, kbh = half(q), half(k), half(kb)
+            kh, kbh = half(k), half(kb)
             grow = jnp.exp(cumc)
             last = cumc[span - 1 :, :]
             right = jnp.concatenate([v * beta, kb * grow], axis=1)
-            low_off, sc_diag, sc_off = [], [], []
+            low_off = []
             for i in range(nblk):
                 at = slice(i * BLOCK, (i + 1) * BLOCK)
                 diff = cumc[at] - cumr[:, at]
                 w_d = jnp.where(causal, jnp.exp(jnp.where(causal, diff, 0.0)), 0.0)
                 diags.append(jnp.where(row > col, dot(kbh[at], kh[at], NT) * w_d, 0.0))
-                sc_diag.append(half(dot(qh[at], kh[at], NT) * w_d))
                 if i:
                     before = slice(0, i * BLOCK)
                     w_o = jnp.exp(cumc[at] - cumr[:, before])
                     low_off.append(half(dot(kbh[at], kh[before], NT) * w_o))
-                    sc_off.append(half(dot(qh[at], kh[before], NT) * w_o))
             per_head.append(
-                dict(right=right, low=low_off, scd=sc_diag, sco=sc_off, qg=q * grow, last=last,
-                     kdec=half(k * jnp.exp(last - cumc)))
+                dict(right=half(right), low=low_off, last=last, kdec=half(k * jnp.exp(last - cumc)))
             )
         hook()
         inv = unit_lower_inverses(diags)
-        hook2()
         done = [[] for _ in range(heads)]
+        own, cross = {}, {}
         for i in range(nblk):
             at = slice(i * BLOCK, (i + 1) * BLOCK)
             for h in range(heads):
-                e = per_head[h]
-                rhs = e["right"][at]
+                e, t = per_head[h], inv[h * nblk + i]
+                own[h, i] = dot(t, e["right"][at])
                 if i:
-                    rhs = rhs - dot(e["low"][i - 1], jnp.concatenate(done[h], axis=0) if i > 1 else done[h][0])
-                done[h].append(half(dot(inv[h * nblk + i], half(rhs))))
+                    cross[h, i] = half(dot(t, e["low"][i - 1]))
+        for i in range(nblk):
+            for h in range(heads):
+                u = own[h, i]
+                if i:
+                    u = u - dot(cross[h, i], jnp.concatenate(done[h], axis=0) if i > 1 else done[h][0])
+                done[h].append(half(u))
         eye = iota((extent, extent), 0) == iota((extent, extent), 1)
         for h in range(heads):
             e = per_head[h]
             uw = jnp.concatenate(done[h], axis=0)
+            r.ubuf[s, h] = uw
             fin = dot(uw, e["kdec"], TN)
             step = half(jnp.where(eye, jnp.exp(e["last"]) - 1.0, 0.0) - fin[extent:])
             state = half(fin[:extent])
@@ -326,16 +342,26 @@
         for d in (2, 1, 3):
             x_copy(s, peer_x(d)).start()
         r.in1[s, x] = r.out1[s, x]
-
+        after()
+
+    def outputs_of(s):
+        causal = iota((BLOCK, BLOCK), 0) >= iota((BLOCK, BLOCK), 1)
         for h in range(heads):
-            e = per_head[h]
+            lanes = slice(h * extent, (h + 1) * extent)
+            q = unit_rows(r.rows[s, 0, :, lanes].astype(f32))
+            kh = half(unit_rows(r.rows[s, 1, :, lanes].astype(f32)))
+            cumc, cumr = r.cum_col[s, :, h : h + 1], r.cum_row[s, h : h + 1, :]
+            qh, qg = half(q), q * jnp.exp(cumc)
             for i in range(nblk):
-                at = slice(i * BLOCK, (i + 1) * BLOCK)
-                out = dot(e["scd"][i], done[h][i])
+                at, before = slice(i * BLOCK, (i + 1) * BLOCK), slice(0, i * BLOCK)
+                diff = cumc[at] - cumr[:, at]
+                w_d = jnp.where(causal, jnp.exp(jnp.where(causal, diff, 0.0)), 0.0)
+                out = dot(half(dot(qh[at], kh[at], NT) * w_d), r.ubuf[s, h, at])
                 if i:
-                    out = out + dot(e["sco"][i - 1], jnp.concatenate(done[h][:i], axis=0) if i > 1 else done[h][0])
+                    w_o = jnp.exp(cumc[at] - cumr[:, before])
+                    out = out + dot(half(dot(qh[at], kh[before], NT) * w_o), r.ubuf[s, h, before])
                 r.local_out[s, h, at, :] = out[:, :extent]
-                r.reach[s, h, at, :] = half(e["qg"][at] - out[:, extent:])
+                r.reach[s, h, at, :] = half(qg[at] - out[:, extent:])
             gate = r.rows[s, 3, :, h * extent : (h + 1) * extent].astype(f32)
             r.gated[s, h] = gate * jax.nn.sigmoid(gate) * r.gain[...]
 
@@ -495,7 +521,7 @@
     tails = jnp.logical_or(z == GROUP, z == 2 * GROUP - 1)
 
     def tail_z(i):
-        return jnp.where(z == GROUP, 2 + i, lax.rem(6 + i, 2 * GROUP))
+        return jnp.where(z == GROUP, (3, 2, 5, 4)[i], (0, 1, 6, 7)[i])
 
     def tail_copy(s, i, xx):
         return pltpu.make_async_remote_copy(
@@ -504,8 +530,11 @@
             device_id=sp_id(tail_z(i), xx), device_id_type=MESH,
         )
 
-    def tail_self(i, xx):
-        return jnp.logical_and(tail_z(i) == z, x == xx)
+    def tail_each(s, act):
+        for i in range(GROUP):
+            for d in (2, 1, 3, 0):
+                if i < GROUP - 1 or d:
+                    act(tail_copy(s, i, peer_x(d)))
 
     def prepare_read(s):
         shape = r.nq.shape
@@ -539,16 +568,8 @@
             for xx in range(GROUP):
                 r.tail_out[s, i * GROUP + xx, 0:4] = keys[xx * 4 : xx * 4 + 4]
                 r.tail_out[s, i * GROUP + xx, 4:8] = answer
-        for i in range(GROUP):
-            for xx in range(GROUP):
-
-                @pl.when(tail_self(i, xx))
-                def _():
-                    r.tail_in[s, x] = r.tail_out[s, i * GROUP + xx]
-
-                @pl.when(jnp.logical_not(tail_self(i, xx)))
-                def _():
-                    tail_copy(s, i, xx).start()
+        tail_each(s, lambda copy: copy.start())
+        r.tail_in[s, x] = r.tail_out[s, (GROUP - 1) * GROUP + x]
 
     def upper(s):
         @pl.when(jnp.logical_not(lower_quad))
@@ -559,11 +580,12 @@
             ).wait_recv()
             s4h = r.s4_in[s]
             s4 = s4h.astype(f32)
-            give_states(s, [s4 + dot(s4h, r.comp_d[s, j]) + r.comp_c[s, j] for j in range(GROUP)])
 
             @pl.when(tails)
             def _():
                 tail(s, s4, s4h)
+
+            give_states(s, [s4 + dot(s4h, r.comp_d[s, j]) + r.comp_c[s, j] for j in range(GROUP)])
 
     def finish(s):
         for o in range(GROUP):
@@ -602,6 +624,9 @@
     def phase(name, step, *args):
         with jax.named_scope(name):
             step(*args)
+
+    def nothing():
+        pass
 
     def group0_early():
         pl.semaphore_wait(r.relay_z.at[1], 2)
@@ -615,16 +640,16 @@
     phase("own1a", start_own, 1, 0)
     phase("cf0", cross_first, 0)
     phase("u0b", use, [0], [(3, 0), (5, 1), (2, 1), (4, 0)])
+    phase("own1b", start_own, 1, 1)
     phase("far0", far, 0)
-    phase("own1b", start_own, 1, 1)
     phase("cs0", cross_second, 0)
     phase("u0c", use, [0], [(3, 1), (5, 0), (6, 0), (6, 1)])
+    phase("nf1", near_first, 1)
     phase("cfar0", cross_far, 0)
     phase("u0d", use, [0], [(7, 0), (7, 1)])
     phase("rows0", round_rows, 0)
-    phase("local0", local, 0, lambda: phase("nf1", near_first, 1), lambda: phase("ns1", near_second, 1))
+    phase("local0", local, 0, lambda: phase("ns1", near_second, 1), lambda: phase("far1", far, 1))
     phase("u1a", use, [1], [(2, 0), (4, 1), (2, 1), (4, 0)])
-    phase("far1", far, 1)
     phase("cc1", cross_first, 1)
     phase("cs1", cross_second, 1)
     phase("u1b", use, [1], [(3, 0), (5, 1), (3, 1), (5, 0)])
@@ -632,9 +657,15 @@
     phase("cfar1", cross_far, 1)
     phase("u1d", use, [1], [(7, 0), (7, 1)])
     phase("rows1", round_rows, 1)
-    phase("local1", local, 1, group0_early, lambda: None)
+    phase("local1", local, 1, nothing, group0_early)
     for s in range(seqs):
-        phase(f"prep{s}", prepare_read, s)
+        phase(f"outs{s}", outputs_of, s)
+
+    @pl.when(tails)
+    def _():
+        for s in range(seqs):
+            prepare_read(s)
+
     phase("group1", combine_group, 1)
     phase("quad0", combine_quad, 0)
     phase("upper0", upper, 0)
@@ -666,12 +697,28 @@
 
         @pl.when(tails)
         def _():
-            for i in range(GROUP):
-                for xx in range(GROUP):
-
-                    @pl.when(jnp.logical_not(tail_self(i, xx)))
-                    def _():
-                        tail_copy(s, i, xx).wait_send()
+            tail_each(s, lambda copy: copy.wait_send())
+
+
+def put_kernel(*refs):
+    sems = refs[6]
+    copies = [pltpu.make_async_copy(refs[i], refs[3 + i], sems.at[i]) for i in range(3)]
+    for copy in copies:
+        copy.start()
+    for copy in copies:
+        copy.wait()
+
+
+def put(arrays):
+    return pl.pallas_call(
+        put_kernel,
+        out_shape=tuple(jax.ShapeDtypeStruct(a.shape, a.dtype) for a in arrays),
+        in_specs=[pl.BlockSpec(memory_space=pltpu.VMEM)] * 3,
+        out_specs=(pl.BlockSpec(memory_space=pltpu.HBM),) * 3,
+        scratch_shapes=[pltpu.SemaphoreType.DMA((3,))],
+        compiler_params=pltpu.CompilerParams(vmem_limit_bytes=2 * 1024 * 1024),
+        name="put",
+    )(*arrays)
 
 
 def shards(
@@ -712,6 +759,9 @@
         acc=pltpu.VMEM((4, seqs * span, width), f32),
         sacc=pltpu.VMEM((seqs, 2 * PAD, span), f32),
         rows=pltpu.VMEM((seqs, 4, span, width), bf16),
+        cum_row=pltpu.VMEM((seqs, PAD, span), f32),
+        cum_col=pltpu.VMEM((seqs, span, PAD), f32),
+        ubuf=pltpu.VMEM((seqs, heads, span, 2 * extent), bf16),
         local_out=pltpu.VMEM((seqs, heads, span, extent), f32),
         reach=pltpu.VMEM((seqs, heads, span, extent), bf16),
         gated=pltpu.VMEM((seqs, heads, span, extent), f32),
@@ -758,7 +808,7 @@
     def body(*refs):
         fused_kernel(names, dims, *refs)
 
-    return pl.pallas_call(
+    results = pl.pallas_call(
         body,
         out_shape=tuple(outputs.values()),
         in_specs=[hbm] * len(inputs),
@@ -777,6 +827,7 @@
             )
         )
     )
+    return put(results)
 
 
 def solution(mesh):

time: 53.6 us -> 49.5 us (0.924)
  Pallas kernels: 51.1 us -> 48.8 us
  local copies, waits for them, and re-layouts: 1.85 us -> 0 us
    pallas_call x1, Pallas kernels: 51.1 us -> 48.1 us  [shards(): pl.pallas_call(body, out_shape=tuple(outputs.values()), in_specs=[hbm] *...]
    unnamed x3 -> x0, local copies, waits for them, and re-layouts: 1.85 us -> none
    pallas_call x0 -> x1, Pallas kernels: none -> 0.71 us  [put(): pl.pallas_call(put_kernel, out_shape=tuple((jax.ShapeDtypeStruct(a.shape,...]
where the time goes in v3:
time: 49.5 us; the launch traced here: 49.4 us
  Pallas kernels  48.8 us (99%)
  between operations  0.64 us (1%)
    pallas_call x1, Pallas kernels, shards(): pl.pallas_call(body, out_shape=tuple(outputs.values()), in_specs=[hbm] *...  48.1 us

profile of v3, /device:TPU:32, one launch (start us, length us, event | category | flops | bytes accessed | tf_op | source)
XLA Modules:
  0.0 49.4 jit_solution(6059665243072630190)
XLA Ops:
  0.6 48.1 %fused.1 = (bf16[2,192,256]{2,1,0:T(8,128)(2,1)S(1)}, bf16[2,2,4,128]{3,2,1,0:T(4,128)(2,1)S(1)}, f32[2,256]{1,0:T(2,128)S(1)}) custom-call(bf16[2,192,512]{2,1,0:T(8,128)(2,1)} %refs_0_.1, bf16[4096,256]{1,0:T(8,128)(2,1)} %refs_1_.1, bf16[4096,256]{1,0:T(8,128)(2,1)} %refs_2_.1, bf16[4096,256]{1,0:T(8,128)(2,1)} %refs_3_.1, bf16[4096,256]{1,0:T(8,128)(2,1)} %refs_4_.1, ...), custom_call_target="tpu_custom_call" | custom-call | tf_op jit(solution)/shard_map/fused/pallas_call | solution.py:811
  48.7 0.7 %put.1 = (bf16[2,192,256]{2,1,0:T(8,128)(2,1)}, bf16[2,2,4,128]{3,2,1,0:T(4,128)(2,1)}, f32[2,256]{1,0:T(2,128)}) custom-call(bf16[2,192,256]{2,1,0:T(8,128)(2,1)S(1)} %get-tuple-element.6.refs_0_, bf16[2,2,4,128]{3,2,1,0:T(4,128)(2,1)S(1)} %get-tuple-element.7.refs_1_, f32[2,256]{1,0:T(2,128)S(1)} %get-tuple-element.8.refs_2_), custom_call_target="tpu_custom_call" | custom-call | tf_op jit(solution)/shard_map/put/pallas_call | solution.py:713
